TPU v7x, 256 devices: a whole 4x4x8 slice. The times are simulated.
256 devices in a mesh: ep: 64 (over z, x, core), tp: 4 (over y).
Axes of the slice: x: 4, y: 4, z: 8, core: 2. Of those that a mesh axis runs over, the one named last changes fastest.
Arguments:
- query_latent: bfloat16 [8192, 512], P('ep'), may hold values from -6 to 6
- key_latent: bfloat16 [8192, 256], P('ep'), may hold values from -6 to 6
- rope_key: bfloat16 [8192, 64], P('ep'), may hold values from -500 to 500
- query_gain: float32 [512], replicated, may hold values from 0.1 to 1.9
- key_gain: float32 [256], replicated, may hold values from 0.1 to 1.9
- w_query: bfloat16 [512, 1024], P(None, 'tp'), may hold values from -0.25 to 0.25
- w_query_rope: bfloat16 [512, 512], P(None, 'tp'), may hold values from -0.25 to 0.25
- w_key: bfloat16 [256, 1024], P(None, 'tp'), may hold values from -0.375 to 0.375
- w_value: bfloat16 [256, 1024], P(None, 'tp'), may hold values from -0.375 to 0.375
- w_out: bfloat16 [1024, 2048], P('tp'), may hold values from -1.796875 to 1.796875
- tokens_b: bfloat16 [32768, 2048], P('ep'), may hold values from -6 to 6
- ffn_gain: float32 [2048], replicated, may hold values from 0.1 to 1.9
- route_expert: int32 [32768, 2], P('ep'), may hold values from 0 to 63, as said below
- route_weight: float32 [32768, 2], P('ep'), may hold values from 0.2 to 1
- w_gate: bfloat16 [64, 2048, 1024], P('ep', None, 'tp'), may hold values from -0.125 to 0.125
- w_up: bfloat16 [64, 2048, 1024], P('ep', None, 'tp'), may hold values from -0.125 to 0.125
- w_down: bfloat16 [64, 1024, 2048], P('ep', 'tp'), may hold values from -0.1875 to 0.1875
Outputs:
- mixer_out: bfloat16 [8192, 2048], P(('ep', 'tp'))
- moe_out: bfloat16 [32768, 2048], P('ep', 'tp')
Inputs may be any that keep to these rules, and one draw needn't show every extreme that they name: `route_expert`: expert e belongs to group e // 16. A row's 2 experts differ and lie in one group. Among the rows of one device along ep, every group is named by exactly 128 rows and every expert is named exactly 16 times.
All inputs are finite; a program needn't handle non-finite values.
Results may differ from a plain program's by a relative error of at most 0.013.
The roundings to bfloat16 on the way count: a program that leaves them out, or rounds other values in their place, can miss the bound.
Values may be sent and summed in bfloat16 or wider, within the bound.
No kernel may reach another device: no remote copies, remote signals or barrier semaphores. Data moves between devices by JAX's collectives and lax.ppermute only.
A program may use at most 64 MiB of HBM per device.

v0:
```python
import functools
import math

import jax
import jax.numpy as jnp
import numpy as np
from jax import lax
from jax.experimental import pallas as pl
from jax.experimental.pallas import tpu as pltpu
from jax.sharding import Mesh
from jax.sharding import PartitionSpec as P

NOPE = 128
ROPE = 64
VDIM = 128
GRID_W = 64
TOPK = 2
EP = ("z", "x", "c")
TP = ("yh", "yl")

epsilon = 1e-06
rotary_base = 10000.0
neg_large = -1e30
f32 = jnp.float32
bf16 = jnp.bfloat16


def params(mib):
    return pltpu.CompilerParams(vmem_limit_bytes=mib * 1024 * 1024)


def dot_t(a, b):
    return lax.dot_general(a, b, (((1,), (1,)), ((), ())), preferred_element_type=f32)


def dot_0(a, b):
    return lax.dot_general(a, b, (((0,), (0,)), ((), ())), preferred_element_type=f32)


def dot(a, b):
    return jnp.dot(a, b, preferred_element_type=f32)


def iota(shape, dim):
    return lax.broadcasted_iota(jnp.int32, shape, dim)


def rms(widened, gain):
    normed = widened * lax.rsqrt(jnp.mean(widened * widened, axis=-1, keepdims=True) + epsilon)
    return (normed * gain).astype(bf16)


def swap_matrix(n):
    row, col = iota((n, n), 0), iota((n, n), 1)
    minus = (row == col + 1) & (col % 2 == 0)
    plus = (row + 1 == col) & (col % 2 == 1)
    return (jnp.where(plus, 1.0, 0.0) - jnp.where(minus, 1.0, 0.0)).astype(bf16)


def latent_kernel(kl_ref, rk_ref, kg_ref, cos_ref, sin_ref, send_ref):
    normed = rms(kl_ref[...].astype(f32), kg_ref[...])
    turned = rk_ref[...].astype(f32) * cos_ref[...] + dot(rk_ref[...], swap_matrix(ROPE)) * sin_ref[...]
    ways = normed.shape[1] // ROPE
    few = normed.shape[0] // ways
    turned = turned.astype(bf16)
    lined = jnp.concatenate([turned[q * few : (q + 1) * few, :] for q in range(ways)], axis=1)
    send_ref[: normed.shape[0]] = normed
    send_ref[normed.shape[0] :] = lined


def join_kernel(*refs):
    out_ref = refs[-1]
    for i, ref in enumerate(refs[:-1]):
        out_ref[i] = ref[...]


def query_kernel(ql_ref, qg_ref, wq_ref, wqr_ref, cos_ref, sin_ref, q_ref):
    heads = q_ref.shape[0]
    normed = rms(ql_ref[...].astype(f32), qg_ref[...])
    nope = dot(normed, wq_ref[...]).astype(bf16)
    swapped = dot(wqr_ref[...], swap_matrix(heads * ROPE)).astype(bf16)
    plain = dot(normed, wqr_ref[...])
    other = dot(normed, swapped)
    for h in range(heads):
        at = slice(h * ROPE, (h + 1) * ROPE)
        rot = (plain[:, at] * cos_ref[...] + other[:, at] * sin_ref[...]).astype(bf16)
        q_ref[h] = jnp.concatenate([nope[:, h * NOPE : (h + 1) * NOPE], rot, jnp.zeros(rot.shape, bf16)], axis=1)


def attend_kernel(count, me_ref, q_ref, wk_ref, wv_ref, wo_ref, *refs):
    kv_refs, refs = refs[:count], refs[count:]
    out_refs, (kv_ref, all_ref, m_ref, l_ref, acc_ref, sem) = refs[:-6], refs[-6:]
    heads, tok_rows = q_ref.shape[:2]
    rank = wk_ref.shape[0]
    scale = (NOPE + ROPE) ** (-0.5)
    loads = [pltpu.make_async_copy(ref, kv_ref.at[i], sem.at[i]) for i, ref in enumerate(kv_refs)]
    for load in loads:
        load.start()
    m_ref[...] = jnp.full(m_ref.shape, neg_large, f32)
    l_ref[...] = jnp.zeros(l_ref.shape, f32)
    acc_ref[...] = jnp.zeros(acc_ref.shape, f32)
    blocks = kv_ref.shape[1]
    ways = rank // ROPE
    few = tok_rows // ways

    def step(j, carry):
        latent, turned = [], []
        for i in (2 * j, 2 * j + 1):
            pltpu.make_async_copy(kv_ref.at[i], kv_ref.at[i], sem.at[i]).wait()
            for q in range(ways):
                latent.append(kv_ref[i, :, q * few : (q + 1) * few, :].reshape(blocks * few, rank))
                part = kv_ref[i, :, tok_rows:, q * ROPE : (q + 1) * ROPE].reshape(blocks * few, ROPE)
                turned.append(jnp.concatenate([part, jnp.zeros(part.shape, bf16)], axis=1))
        latent = jnp.concatenate(latent, axis=0)
        turned = jnp.concatenate(turned, axis=0)
        keys = dot(latent, wk_ref[...]).astype(bf16)
        values = dot(latent, wv_ref[...]).astype(bf16)
        for h in range(heads):
            both = jnp.concatenate([keys[:, h * NOPE : (h + 1) * NOPE], turned], axis=1)
            scores = dot_t(both, q_ref[h]) * scale
            old = m_ref[h : h + 1, :]
            new = jnp.maximum(old, jnp.max(scores, axis=0, keepdims=True))
            weights = jnp.exp(scores - new)
            shrink = jnp.exp(old - new)
            m_ref[h : h + 1, :] = new
            l_ref[h : h + 1, :] = l_ref[h : h + 1, :] * shrink + jnp.sum(weights, axis=0, keepdims=True)
            added = dot_0(values[:, h * VDIM : (h + 1) * VDIM], weights.astype(bf16))
            acc_ref[h] = acc_ref[h] * shrink + added
        return carry

    lax.fori_loop(0, count // 2, step, 0)
    parts = [(acc_ref[h] / l_ref[h : h + 1, :]).astype(bf16) for h in range(heads)]
    all_ref[...] = dot_0(jnp.concatenate(parts, axis=0), wo_ref[...]).astype(bf16)
    share = tok_rows // len(out_refs)
    for k, out_ref in enumerate(out_refs):
        owner = lax.rem(me_ref[0] + k, len(out_refs))
        out_ref[...] = all_ref[pl.ds(pl.multiple_of(owner * share, share), share), :]


def rotary_lanes(tok_rows):
    positions = lax.axis_index(EP) * tok_rows + jnp.arange(tok_rows, dtype=jnp.int32)
    half = ROPE // 2
    inverse = rotary_base ** (-np.arange(0, half, 2, dtype=np.float32) / half)
    pair = np.arange(ROPE) // 2
    spread = jnp.asarray(inverse.astype(np.float32)[pair % (half // 2)])
    by_row = jnp.asarray(pair < half // 2)
    grid_row = (positions // GRID_W).astype(f32)
    grid_col = (positions % GRID_W).astype(f32)
    angle = jnp.where(by_row[None, :], grid_row[:, None], grid_col[:, None]) * spread[None, :]
    return jnp.cos(angle), jnp.sin(angle)


def prep_kernel(me_ref, tok_hbm, gain_hbm, route_hbm, target_ref, out_hbm, *scratch):
    tok_ref, gain_ref, route_ref, normed_ref, out_ref, load_sem, store_sem = scratch
    tok_rows, _ = tok_ref.shape
    part = normed_ref.shape[1]
    experts, per = out_ref.shape[:2]
    upper = me_ref[0] // 2
    half = (me_ref[0] // 2 + me_ref[0]) % 2
    at = pl.ds(pl.multiple_of(upper * part, part), part)
    blocks = 4
    block = tok_rows // blocks
    loads = [
        pltpu.make_async_copy(route_hbm, route_ref, load_sem.at[0]),
        pltpu.make_async_copy(gain_hbm, gain_ref, load_sem.at[1]),
    ]
    for i in range(blocks):
        rows = pl.ds(i * block, block)
        loads.append(pltpu.make_async_copy(tok_hbm.at[rows], tok_ref.at[rows], load_sem.at[2 + i]))
    for load in loads:
        load.start()

    loads[0].wait()
    names = iota((128, tok_rows), 0)
    first, second = route_ref[0:1, :], route_ref[1:2, :]
    named = (names == first) | (names == second)
    before = iota((tok_rows, tok_rows), 0) < iota((tok_rows, tok_rows), 1)
    earlier = dot(named.astype(bf16), before.astype(bf16))
    for c, chosen in enumerate((first, second)):
        slot = jnp.sum(jnp.where(names == chosen, earlier, 0.0), axis=0, keepdims=True).astype(jnp.int32)
        sender = (slot // per + upper) % 2
        target_ref[c : c + 1, :] = (chosen * 2 + sender) * per + slot % per
    code = jnp.where(named, earlier, -1.0).astype(bf16)

    loads[1].wait()
    for i in range(blocks):
        loads[2 + i].wait()
        rows = slice(i * block, (i + 1) * block)
        widened = tok_ref[rows, :].astype(f32)
        scale = lax.rsqrt(jnp.mean(widened * widened, axis=-1, keepdims=True) + epsilon)
        mine = tok_ref[rows, at].astype(f32)
        normed_ref[rows, :] = ((mine * scale) * gain_ref[:, at]).astype(bf16)

    share = experts // 2
    rows_out = share * per
    stores = []
    for i in range(2):
        owner = (iota((rows_out, 128), 0) // per + i * share == iota((rows_out, 128), 1)).astype(bf16)
        spread = dot(owner, code)
        within = iota((rows_out, tok_rows), 0) % per + half * per
        pick = (spread == within.astype(f32)).astype(bf16)
        out_ref[i * share : (i + 1) * share] = dot(pick, normed_ref[...]).astype(bf16).reshape(share, per, part)
        which = pl.ds(i * share, share)
        stores.append(pltpu.make_async_copy(out_ref.at[which], out_hbm.at[which], store_sem.at[i]))
        stores[-1].start()
    for store in stores:
        store.wait()


def half_kernel(me_ref, a_ref, wg_ref, wu_ref, vg_ref, vu_ref, *out_refs):
    part = a_ref.shape[1]
    units = wg_ref.shape[1]
    rows = out_refs[0].shape[0]
    at = pl.ds(pl.multiple_of(me_ref[0] // 2 * part, part), part)
    for i, out_ref in enumerate(out_refs):
        for k, ref in enumerate((wg_ref, wu_ref, vg_ref, vu_ref)):
            out_ref[:, k * units : (k + 1) * units] = dot(a_ref[i * rows : (i + 1) * rows, :], ref[at, :])


def hidden_kernel(me_ref, b_ref, wg_ref, wu_ref, vg_ref, vu_ref, held_ref, out_ref):
    part = b_ref.shape[1]
    units = wg_ref.shape[1]
    at = pl.ds(pl.multiple_of((1 - me_ref[0] // 2) * part, part), part)
    for k, (g_ref, u_ref) in enumerate(((wg_ref, wu_ref), (vg_ref, vu_ref))):
        cols = 2 * k * units
        gate = held_ref[:, cols : cols + units] + dot(b_ref[...], g_ref[at, :])
        up = held_ref[:, cols + units : cols + 2 * units] + dot(b_ref[...], u_ref[at, :])
        out_ref[:, k * units : (k + 1) * units] = (gate * (1.0 / (1.0 + jnp.exp(-gate))) * up).astype(bf16)


def split_kernel(me_ref, wd_ref, mine_ref, other_ref):
    part = mine_ref.shape[1]
    upper = me_ref[0] // 2
    mine_ref[...] = wd_ref[:, pl.ds(pl.multiple_of(upper * part, part), part)]
    other_ref[...] = wd_ref[:, pl.ds(pl.multiple_of((1 - upper) * part, part), part)]


def down_kernel(a_ref, b_ref, w0_ref, w1_ref, w2_ref, w3_ref, *rest):
    out_ref = rest[-1]
    units = w0_ref.shape[0]
    experts, ways, per, part = out_ref.shape
    fresh = a_ref.shape[0] // per
    if len(rest) > 1:
        out_ref[: experts - fresh] = rest[0][...]
    for y in range(ways):
        cols = slice(y * part, (y + 1) * part)
        total = 0.0
        for ref, k, wd_ref in ((a_ref, 0, w0_ref), (a_ref, 1, w1_ref), (b_ref, 0, w2_ref), (b_ref, 1, w3_ref)):
            term = dot(ref[:, k * units : (k + 1) * units], wd_ref[:, cols])
            total = total + term.astype(bf16).astype(f32)
        out_ref[experts - fresh :, y] = total.astype(bf16).reshape(fresh, per, part)


def combine_kernel(target_ref, weight_ref, *rest):
    ret_refs, out_ref = rest[:-1], rest[-1]
    rows = ret_refs[0].shape[0]
    tok_rows = out_ref.shape[0]
    total = 0.0
    lanes = iota((tok_rows, rows), 1)
    for c in range(TOPK):
        target = target_ref[:, c : c + 1]
        picked = 0.0
        for k, ref in enumerate(ret_refs):
            pick = (lanes == target - k * rows).astype(bf16)
            picked = picked + dot(pick, ref[...])
        total = total + picked * weight_ref[:, c : c + 1]
    out_ref[...] = total.astype(bf16)


def smem():
    return pl.BlockSpec(memory_space=pltpu.SMEM)


def vmem():
    return pl.BlockSpec(memory_space=pltpu.VMEM)


def call(kernel, out_shape, args, flops, scratch=(), mib=48):
    outs = out_shape if isinstance(out_shape, (tuple, list)) else (out_shape,)
    moved = sum(a.size * a.dtype.itemsize for a in args) + sum(
        math.prod(o.shape) * o.dtype.itemsize for o in outs
    )
    return pl.pallas_call(
        kernel,
        out_shape=out_shape,
        in_specs=[smem() if a.size == 1 else vmem() for a in args],
        out_specs=jax.tree.map(lambda _: vmem(), out_shape),
        scratch_shapes=list(scratch),
        compiler_params=params(mib),
        cost_estimate=pl.CostEstimate(flops=flops, transcendentals=0, bytes_accessed=moved),
    )(*args)


def shape(*dims, dtype=bf16):
    return jax.ShapeDtypeStruct(dims, dtype)


def inner(
    query_latent,
    key_latent,
    rope_key,
    query_gain,
    key_gain,
    w_query,
    w_query_rope,
    w_key,
    w_value,
    w_out,
    tokens_b,
    ffn_gain,
    route_expert,
    route_weight,
    w_gate,
    w_up,
    w_down,
):
    tp = lax.axis_size(TP)
    experts = lax.axis_size(EP)
    me = lax.axis_index(TP).astype(jnp.int32).reshape(1)

    def ahead(k, n=tp):
        return [(i, (i + k) % n) for i in range(n)]

    def across(k):
        return [(i, i ^ k) for i in range(tp)]

    far_gate = lax.ppermute(w_gate[0], TP, across(1))
    far_up = lax.ppermute(w_up[0], TP, across(1))

    tok_b, width = tokens_b.shape
    per = TOPK * tok_b // experts // 2
    part = width // 2
    rows = experts * per
    units = w_gate.shape[2]
    far = pl.BlockSpec(memory_space=pltpu.HBM)
    target, outgoing = pl.pallas_call(
        prep_kernel,
        out_shape=[shape(TOPK, tok_b, dtype=jnp.int32), shape(experts, per, part)],
        in_specs=[smem(), far, far, far],
        out_specs=[vmem(), far],
        scratch_shapes=[
            pltpu.VMEM((tok_b, width), bf16),
            pltpu.VMEM((1, width), f32),
            pltpu.VMEM((TOPK, tok_b), jnp.int32),
            pltpu.VMEM((tok_b, part), bf16),
            pltpu.VMEM((experts, per, part), bf16),
            pltpu.SemaphoreType.DMA((6,)),
            pltpu.SemaphoreType.DMA((2,)),
        ],
        compiler_params=params(48),
        cost_estimate=pl.CostEstimate(flops=6 * 10**8, transcendentals=0, bytes_accessed=4 * 10**6),
        name="prep",
    )(me, tokens_b, ffn_gain.reshape(1, -1), route_expert.T)
    arrived = lax.all_to_all(outgoing, EP, 0, 0, tiled=True)
    arrived = arrived.reshape(rows, part)

    mine, other = call(split_kernel, [shape(units, part)] * 2, (me, w_down[0]), 10**6)
    down3 = lax.ppermute(other, TP, across(3))
    down1 = lax.ppermute(mine, TP, across(1))
    down2 = lax.ppermute(down3, TP, across(1))
    down = (mine, down1, down3, down2)

    tok_a = query_latent.shape[0]
    heads = w_query.shape[1] // NOPE
    cosine, sine = rotary_lanes(tok_a)
    rank = key_latent.shape[1]
    sent = tok_a + tok_a * ROPE // rank
    depth = lax.axis_size("z")
    send = call(latent_kernel, shape(sent, rank), (key_latent, rope_key, key_gain.reshape(1, -1), cosine, sine), 10**7)
    wide = lax.axis_size("x")
    row = [send]
    for k in range(1, wide):
        row.append(lax.ppermute(send, "x", ahead(k, wide)))
    row = call(join_kernel, shape(wide, sent, rank), tuple(row), 10**6)
    queries = call(
        query_kernel,
        shape(heads, tok_a, NOPE + 2 * ROPE),
        (query_latent, query_gain.reshape(1, -1), w_query, w_query_rope, cosine, sine),
        10**8,
    )

    halves = 2
    few = rows // halves
    weights = (w_gate[0], w_up[0], far_gate, far_up)
    joined = []
    for i in range(halves):
        joined.append(lax.ppermute(arrived[i * few : (i + 1) * few], TP, across(3)))
    held = call(
        half_kernel, [shape(few, 4 * units, dtype=f32)] * halves, (me, arrived, *weights), 8 * rows * part * units
    )
    result = ()
    for i in range(halves):
        hidden = call(hidden_kernel, shape(few, 2 * units), (me, joined[i], *weights, held[i]), 8 * few * part * units)
        far_hidden = lax.ppermute(hidden, TP, across(3))
        result = (
            call(
                down_kernel,
                shape(experts * (i + 1) // halves, 2, per, part // 2),
                (hidden, far_hidden, *down, *result),
                8 * few * units * part,
            ),
        )
    result = result[0]

    near = [row]
    up, low = row, row
    for k in range(1, depth // 2 + 1):
        up = lax.ppermute(up, "z", ahead(1, depth))
        near.append(up)
        if 2 * k < depth:
            low = lax.ppermute(low, "z", ahead(depth - 1, depth))
            near.append(low)
    pieces = []
    for piece in near[:depth]:
        pieces += [piece, lax.ppermute(piece, "c", [(0, 1), (1, 0)])]

    share = shape(tok_a // tp, w_out.shape[1])
    count = len(pieces)
    shares = pl.pallas_call(
        functools.partial(attend_kernel, count),
        out_shape=[share] * tp,
        in_specs=[smem()] + [vmem()] * 4 + [far] * count,
        out_specs=[vmem()] * tp,
        scratch_shapes=[
            pltpu.VMEM((count, *pieces[0].shape), bf16),
            pltpu.VMEM((tok_a, w_out.shape[1]), bf16),
            pltpu.VMEM((heads, tok_a), f32),
            pltpu.VMEM((heads, tok_a), f32),
            pltpu.VMEM((heads, VDIM, tok_a), f32),
            pltpu.SemaphoreType.DMA((count,)),
        ],
        compiler_params=params(48),
        cost_estimate=pl.CostEstimate(flops=6 * 10**9, transcendentals=0, bytes_accessed=8 * 10**6),
        name="attend",
    )(me, queries, w_key, w_value, w_out, *pieces)
    held = [shares[0]] + [lax.ppermute(s, TP, ahead(k)) for k, s in enumerate(shares) if k]
    mixer_out = sum(s.astype(f32) for s in held).astype(bf16)

    returned = lax.all_to_all(result.reshape(2 * experts, per, part // 2), (*EP, "yl"), 0, 0, tiled=True)
    moe_out = call(
        combine_kernel,
        shape(tok_b, part // 2),
        (target.T, route_weight, returned.reshape(2 * rows, part // 2)),
        4 * tok_b * 2 * rows * part // 2,
    )
    return (mixer_out, moe_out)


def spec(*dims):
    spread = {"ep": EP, "tp": TP, "both": EP + TP}
    return P(*(spread.get(d) for d in dims))


def solution(mesh):
    ep, tp = mesh.devices.shape
    fine = Mesh(mesh.devices.reshape(ep // 8, 4, 2, tp // 2, 2), EP + TP)
    in_specs = (
        spec("ep", None),
        spec("ep", None),
        spec("ep", None),
        spec(),
        spec(),
        spec(None, "tp"),
        spec(None, "tp"),
        spec(None, "tp"),
        spec(None, "tp"),
        spec("tp", None),
        spec("ep", None),
        spec(),
        spec("ep", None),
        spec("ep", None),
        spec("ep", None, "tp"),
        spec("ep", None, "tp"),
        spec("ep", "tp", None),
    )
    out_specs = (spec("both", None), spec("ep", "tp"))
    return jax.shard_map(inner, mesh=fine, in_specs=in_specs, out_specs=out_specs, check_vma=False)
```

profile of v0, /device:TPU:1, one launch (start us, length us, event | category | flops | bytes accessed | tf_op | source)
XLA Modules:
  0.0 171.2 jit_solution(4965884894450101967)
XLA Ops:
  0.7 1.6 copy-done.12
  3.7 2.4 %prep.1 = (s32[2,512]{1,0:T(2,128)S(1)}, bf16[64,8,1024]{2,1,0:T(8,128)(2,1)S(1)}) custom-call(s32[1]{0:T(128)} %bitcast.me_ref, bf16[512,2048]{1,0:T(8,128)(2,1)S(1)} %copy-done.12, f32[1,2048]{1,0:T(1,128)S(1)} %bitcast.30, s32[2,512]{1,0:T(2,128)S(1)} %bitcast.31), custom_call_target="tpu_custom_call" | custom-call | flops 600000000 | bytes 4000000 | tf_op jit(solution)/shard_map/prep/pallas_call | solution.py:336
  7.0 13.0 %all-to-all-start = ((bf16[64,8,1024]{2,1,0:T(8,128)(2,1)}), bf16[64,8,1024]{2,1,0:T(8,128)(2,1)S(1)}, u32[]{:S(2)}, u32[]{:S(2)}) async-start(bf16[64,8,1024]{2,1,0:T(8,128)(2,1)} %copy-done.5), calls=%async_computation | async-start | bytes 2097152 | tf_op jit(solution)/shard_map/all_to_all | solution.py:354
  20.0 1.4 collective-permute-start.22
  22.3 1.4 collective-permute-start
  23.7 2.4 %collective-permute-start.1 = (bf16[160,256]{1,0:T(8,128)(2,1)S(1)}, bf16[160,256]{1,0:T(8,128)(2,1)S(1)}, u32[]{:S(2)}, u32[]{:S(2)}) collective-permute-start(bf16[160,256]{1,0:T(8,128)(2,1)S(1)} %shard_map.195.refs_0_), channel_id=1, source_target_pairs={{0,16},{8,24},{16,0},{24,8},{1,17},{9,25},{17,1},{25,9},{2,18},{10... | collective-permute-start | bytes 245768 | tf_op jit(solution)/shard_map/ppermute | solution.py:373
  26.1 1.2 collective-permute-start.2
  27.3 1.2 copy-done.4
  29.4 2.7 %collective-permute-start.26 = (bf16[256,1024]{1,0:T(8,128)(2,1)}, bf16[256,1024]{1,0:T(8,128)(2,1)}, u32[]{:S(2)}, u32[]{:S(2)}) collective-permute-start(bf16[256,1024]{1,0:T(8,128)(2,1)} %get-tuple-element.20), channel_id=1, source_target_pairs={{0,3},{1,2},{2,1},{3,0},{4,7},{5,6},{6,5},{7,4},{8,11},{9,10},{10,... | collective-permute-start | bytes 1572872 | tf_op jit(solution)/shard_map/ppermute | solution.py:358
  32.9 2.3 %collective-permute-start.4 = (bf16[4,160,256]{2,1,0:T(8,128)(2,1)}, bf16[4,160,256]{2,1,0:T(8,128)(2,1)}, u32[]{:S(2)}, u32[]{:S(2)}) collective-permute-start(bf16[4,160,256]{2,1,0:T(8,128)(2,1)} %shard_map.196.refs_0_), channel_id=1, source_target_pairs={{0,32},{32,64},{64,96},{96,128},{128,160},{160,192},{192,224},{224... | collective-permute-start | bytes 983048 | tf_op jit(solution)/shard_map/ppermute | solution.py:408
  35.1 14.6 %all-to-all-done = bf16[64,8,1024]{2,1,0:T(8,128)(2,1)S(1)} async-done(((bf16[64,8,1024]{2,1,0:T(8,128)(2,1)}), bf16[64,8,1024]{2,1,0:T(8,128)(2,1)S(1)}, u32[]{:S(2)}, u32[]{:S(2)}) %all-to-all-start) | async-done | bytes 1048608 | tf_op jit(solution)/shard_map/all_to_all | solution.py:354
  49.8 2.8 %collective-permute-start.28 = (bf16[256,1024]{1,0:T(8,128)(2,1)S(1)}, bf16[256,1024]{1,0:T(8,128)(2,1)S(1)}, u32[]{:S(2)}, u32[]{:S(2)}) collective-permute-start(bf16[256,1024]{1,0:T(8,128)(2,1)S(1)} %get-tuple-element.22), channel_id=1, source_target_pairs={{0,3},{1,2},{2,1},{3,0},{4,7},{5,6},{6,5},{7,4},{8,11},{9,10},{10,... | collective-permute-start | bytes 1572872 | tf_op jit(solution)/shard_map/ppermute | solution.py:387
  53.0 2.7 %collective-permute-start.21 = (bf16[256,1024]{1,0:T(8,128)(2,1)S(1)}, bf16[256,1024]{1,0:T(8,128)(2,1)S(1)}, u32[]{:S(2)}, u32[]{:S(2)}) collective-permute-start(bf16[256,1024]{1,0:T(8,128)(2,1)S(1)} %get-tuple-element.23), channel_id=1, source_target_pairs={{0,3},{1,2},{2,1},{3,0},{4,7},{5,6},{6,5},{7,4},{8,11},{9,10},{10,... | collective-permute-start | bytes 1572872 | tf_op jit(solution)/shard_map/ppermute | solution.py:387
  55.7 1.1 collective-permute-start.6
  56.9 10.1 %collective-permute-done.23.vu_ref = bf16[2048,256]{1,0:T(8,128)(2,1)} collective-permute-done((bf16[2048,256]{1,0:T(8,128)(2,1)S(1)}, bf16[2048,256]{1,0:T(8,128)(2,1)}, u32[]{:S(2)}, u32[]{:S(2)}) %collective-permute-start.23) | collective-permute-done | bytes 1048608 | tf_op jit(solution)/shard_map/ppermute | solution.py:328
  67.0 1.3 collective-permute-start.27
  68.3 1.4 collective-permute-start.8
  69.7 2.8 %shard_map.197 = (f32[256,1024]{1,0:T(8,128)S(1)}, f32[256,1024]{1,0:T(8,128)S(1)}) custom-call(s32[1]{0:T(128)} %bitcast.me_ref, bf16[512,1024]{1,0:T(8,128)(2,1)S(1)} %bitcast.16, bf16[2048,256]{1,0:T(8,128)(2,1)S(1)} %bitcast.18, bf16[2048,256]{1,0:T(8,128)(2,1)S(1)} %bitcast.22, bf16[2048,256]{1,0:T(8,128)(2,1)} %collective-permute-done.22.vg_ref, ...), custom_call_target="tpu_custom_call" | custom-call | flops 1073741824 | bytes 7340036 | tf_op jit(solution)/shard_map/pallas_call | solution.py:283
  72.5 2.3 %shard_map.200.a_ref = bf16[256,512]{1,0:T(8,128)(2,1)S(1)} custom-call(s32[1]{0:T(128)} %bitcast.me_ref, bf16[256,1024]{1,0:T(8,128)(2,1)S(1)} %collective-permute-done.28.b_ref, bf16[2048,256]{1,0:T(8,128)(2,1)S(1)} %bitcast.19, bf16[2048,256]{1,0:T(8,128)(2,1)S(1)} %bitcast.23, bf16[2048,256]{1,0:T(8,128)(2,1)} %collective-permute-done.22.vg_ref, ...), custom_call_target="tpu_custom_call" | custom-call | flops 536870912 | bytes 6029316 | tf_op jit(solution)/shard_map/pallas_call | solution.py:283
  75.8 2.6 %collective-permute-start.29 = (bf16[256,512]{1,0:T(8,128)(2,1)S(1)}, bf16[256,512]{1,0:T(8,128)(2,1)S(1)}, u32[]{:S(2)}, u32[]{:S(2)}) collective-permute-start(bf16[256,512]{1,0:T(8,128)(2,1)S(1)} %shard_map.200.a_ref), channel_id=1, source_target_pairs={{0,3},{1,2},{2,1},{3,0},{4,7},{5,6},{6,5},{7,4},{8,11},{9,10},{10,... | collective-permute-start | bytes 786440 | tf_op jit(solution)/shard_map/ppermute | solution.py:394
  78.5 2.3 %shard_map.198.a_ref = bf16[256,512]{1,0:T(8,128)(2,1)S(1)} custom-call(s32[1]{0:T(128)} %bitcast.me_ref, bf16[256,1024]{1,0:T(8,128)(2,1)S(1)} %collective-permute-done.21.b_ref, bf16[2048,256]{1,0:T(8,128)(2,1)S(1)} %bitcast.20, bf16[2048,256]{1,0:T(8,128)(2,1)S(1)} %bitcast.24, bf16[2048,256]{1,0:T(8,128)(2,1)} %collective-permute-done.22.vg_ref, ...), custom_call_target="tpu_custom_call" | custom-call | flops 536870912 | bytes 6029316 | tf_op jit(solution)/shard_map/pallas_call | solution.py:283
  82.4 6.9 %collective-permute-done.27.w3_ref = bf16[256,1024]{1,0:T(8,128)(2,1)S(1)} collective-permute-done((bf16[256,1024]{1,0:T(8,128)(2,1)}, bf16[256,1024]{1,0:T(8,128)(2,1)S(1)}, u32[]{:S(2)}, u32[]{:S(2)}) %collective-permute-start.27) | collective-permute-done | bytes 524320 | tf_op jit(solution)/shard_map/ppermute | solution.py:360
  89.3 1.8 %shard_map.201.rest_0_ = bf16[32,2,8,512]{3,2,1,0:T(8,128)(2,1)S(1)} custom-call(bf16[256,512]{1,0:T(8,128)(2,1)S(1)} %shard_map.200.a_ref, bf16[256,512]{1,0:T(8,128)(2,1)S(1)} %collective-permute-done.29.b_ref, bf16[256,1024]{1,0:T(8,128)(2,1)S(1)} %copy-done.3, bf16[256,1024]{1,0:T(8,128)(2,1)S(1)} %collective-permute-done.25.w1_ref, ...), custom_call_target="tpu_custom_call" | custom-call | flops 536870912 | bytes 3145728 | tf_op jit(solution)/shard_map/pallas_call | solution.py:283
  91.1 2.8 %shard_map.202 = bf16[64,2,8,512]{3,2,1,0:T(8,128)(2,1)} custom-call(bf16[256,512]{1,0:T(8,128)(2,1)S(1)} %shard_map.198.a_ref, bf16[256,512]{1,0:T(8,128)(2,1)S(1)} %collective-permute-done.24.b_ref, bf16[256,1024]{1,0:T(8,128)(2,1)S(1)} %copy-done.3, bf16[256,1024]{1,0:T(8,128)(2,1)S(1)} %collective-permute-done.25.w1_ref, ...), custom_call_target="tpu_custom_call" | custom-call | flops 536870912 | bytes 4194304 | tf_op jit(solution)/shard_map/pallas_call | solution.py:283
  94.0 13.1 %all-to-all-start.1 = ((bf16[128,8,512]{2,1,0:T(8,128)(2,1)}), bf16[128,8,512]{2,1,0:T(8,128)(2,1)S(1)}, u32[]{:S(2)}, u32[]{:S(2)}) async-start(bf16[128,8,512]{2,1,0:T(8,128)(2,1)} %bitcast.12), calls=%async_computation.1 | async-start | bytes 2097152 | tf_op jit(solution)/shard_map/all_to_all | solution.py:439
  108.6 2.7 %collective-permute-start.14 = (bf16[4,160,256]{2,1,0:T(8,128)(2,1)S(1)}, bf16[4,160,256]{2,1,0:T(8,128)(2,1)S(1)}, u32[]{:S(2)}, u32[]{:S(2)}) collective-permute-start(bf16[4,160,256]{2,1,0:T(8,128)(2,1)S(1)} %collective-permute-done.10.refs_8_), channel_id=1, source_target_pairs={{0,224},{32,0},{64,32},{96,64},{128,96},{160,128},{192,160},{224,1... | collective-permute-start | bytes 983048 | tf_op jit(solution)/shard_map/ppermute | solution.py:411
  112.4 25.6 %collective-permute-done.14.refs_12_ = bf16[4,160,256]{2,1,0:T(8,128)(2,1)S(1)} collective-permute-done((bf16[4,160,256]{2,1,0:T(8,128)(2,1)S(1)}, bf16[4,160,256]{2,1,0:T(8,128)(2,1)S(1)}, u32[]{:S(2)}, u32[]{:S(2)}) %collective-permute-start.14) | collective-permute-done | bytes 327712 | tf_op jit(solution)/shard_map/ppermute | solution.py:411
  142.1 16.4 %attend.1 = (bf16[32,2048]{1,0:T(8,128)(2,1)S(1)}, bf16[32,2048]{1,0:T(8,128)(2,1)S(1)}, bf16[32,2048]{1,0:T(8,128)(2,1)S(1)}, bf16[32,2048]{1,0:T(8,128)(2,1)S(1)}) custom-call(s32[1]{0:T(128)} %bitcast.me_ref, bf16[2,128,256]{2,1,0:T(8,128)(2,1)S(1)} %shard_map.194.q_ref, bf16[256,256]{1,0:T(8,128)(2,1)S(1)} %copy-done.13, ...), custom_call_target="tpu_custom_call" | custom-call | flops 6000000000 | bytes 8000000 | tf_op jit(solution)/shard_map/attend/pallas_call | solution.py:419
  158.5 1.3 collective-permute-start.18
  159.8 2.6 %collective-permute-start.19 = (bf16[32,2048]{1,0:T(8,128)(2,1)S(1)}, bf16[32,2048]{1,0:T(8,128)(2,1)S(1)}, u32[]{:S(2)}, u32[]{:S(2)}) collective-permute-start(bf16[32,2048]{1,0:T(8,128)(2,1)S(1)} %get-tuple-element.14), channel_id=1, source_target_pairs={{0,2},{1,3},{2,0},{3,1},{4,6},{5,7},{6,4},{7,5},{8,10},{9,11},{10,... | collective-permute-start | bytes 393224 | tf_op jit(solution)/shard_map/ppermute | solution.py:436
  164.4 3.9 %collective-permute-done.19 = bf16[32,2048]{1,0:T(8,128)(2,1)S(1)} collective-permute-done((bf16[32,2048]{1,0:T(8,128)(2,1)S(1)}, bf16[32,2048]{1,0:T(8,128)(2,1)S(1)}, u32[]{:S(2)}, u32[]{:S(2)}) %collective-permute-start.19) | collective-permute-done | bytes 131104 | tf_op jit(solution)/shard_map/ppermute | solution.py:436
  169.1 2.1 %shard_map.203 = bf16[512,512]{1,0:T(8,128)(2,1)} custom-call(s32[512,2]{1,0:T(8,128)S(1)} %bitcast.27, f32[512,2]{1,0:T(8,128)S(1)} %copy.23.weight_ref, bf16[1024,512]{1,0:T(8,128)(2,1)S(1)} %bitcast.26), custom_call_target="tpu_custom_call" | custom-call | flops 1073741824 | bytes 1581056 | tf_op jit(solution)/shard_map/pallas_call | solution.py:283
  (93 shorter events, 17.4 us)
Async XLA Ops:
  7.0 42.6 %all-to-all-start = ((bf16[64,8,1024]{2,1,0:T(8,128)(2,1)}), bf16[64,8,1024]{2,1,0:T(8,128)(2,1)S(1)}, u32[]{:S(2)}, u32[]{:S(2)}) async-start(bf16[64,8,1024]{2,1,0:T(8,128)(2,1)} %copy-done.5), calls=%async_computation | async-start | bytes 2097152 | tf_op jit(solution)/shard_map/all_to_all | solution.py:354
  20.0 36.8 %collective-permute-start.22 = (bf16[2048,256]{1,0:T(8,128)(2,1)S(1)}, bf16[2048,256]{1,0:T(8,128)(2,1)}, u32[]{:S(2)}, u32[]{:S(2)}) collective-permute-start(bf16[2048,256]{1,0:T(8,128)(2,1)S(1)} %bitcast.17), channel_id=1, source_target_pairs={{0,1},{1,0},{2,3},{3,2},{4,5},{5,4},{6,7},{7,6},{8,9},{9,8},{10,11... | collective-permute-start | bytes 3145736 | tf_op jit(solution)/shard_map/ppermute | solution.py:327
  21.4 45.5 %collective-permute-start.23 = (bf16[2048,256]{1,0:T(8,128)(2,1)S(1)}, bf16[2048,256]{1,0:T(8,128)(2,1)}, u32[]{:S(2)}, u32[]{:S(2)}) collective-permute-start(bf16[2048,256]{1,0:T(8,128)(2,1)S(1)} %bitcast.21), channel_id=1, source_target_pairs={{0,1},{1,0},{2,3},{3,2},{4,5},{5,4},{6,7},{7,6},{8,9},{9,8},{10,11... | collective-permute-start | bytes 3145736 | tf_op jit(solution)/shard_map/ppermute | solution.py:328
  22.3 7.0 %collective-permute-start = (bf16[160,256]{1,0:T(8,128)(2,1)S(1)}, bf16[160,256]{1,0:T(8,128)(2,1)S(1)}, u32[]{:S(2)}, u32[]{:S(2)}) collective-permute-start(bf16[160,256]{1,0:T(8,128)(2,1)S(1)} %shard_map.195.refs_0_), channel_id=1, source_target_pairs={{0,8},{8,16},{16,24},{24,0},{1,9},{9,17},{17,25},{25,1},{2,10},{10... | collective-permute-start | bytes 245768 | tf_op jit(solution)/shard_map/ppermute | solution.py:373
  23.7 8.4 %collective-permute-start.1 = (bf16[160,256]{1,0:T(8,128)(2,1)S(1)}, bf16[160,256]{1,0:T(8,128)(2,1)S(1)}, u32[]{:S(2)}, u32[]{:S(2)}) collective-permute-start(bf16[160,256]{1,0:T(8,128)(2,1)S(1)} %shard_map.195.refs_0_), channel_id=1, source_target_pairs={{0,16},{8,24},{16,0},{24,8},{1,17},{9,25},{17,1},{25,9},{2,18},{10... | collective-permute-start | bytes 245768 | tf_op jit(solution)/shard_map/ppermute | solution.py:373
  26.1 6.0 %collective-permute-start.2 = (bf16[160,256]{1,0:T(8,128)(2,1)S(1)}, bf16[160,256]{1,0:T(8,128)(2,1)S(1)}, u32[]{:S(2)}, u32[]{:S(2)}) collective-permute-start(bf16[160,256]{1,0:T(8,128)(2,1)S(1)} %shard_map.195.refs_0_), channel_id=1, source_target_pairs={{0,24},{8,0},{16,8},{24,16},{1,25},{9,1},{17,9},{25,17},{2,26},{10... | collective-permute-start | bytes 245768 | tf_op jit(solution)/shard_map/ppermute | solution.py:373
  29.4 26.3 %collective-permute-start.26 = (bf16[256,1024]{1,0:T(8,128)(2,1)}, bf16[256,1024]{1,0:T(8,128)(2,1)}, u32[]{:S(2)}, u32[]{:S(2)}) collective-permute-start(bf16[256,1024]{1,0:T(8,128)(2,1)} %get-tuple-element.20), channel_id=1, source_target_pairs={{0,3},{1,2},{2,1},{3,0},{4,7},{5,6},{6,5},{7,4},{8,11},{9,10},{10,... | collective-permute-start | bytes 1572872 | tf_op jit(solution)/shard_map/ppermute | solution.py:358
  32.9 20.1 %collective-permute-start.4 = (bf16[4,160,256]{2,1,0:T(8,128)(2,1)}, bf16[4,160,256]{2,1,0:T(8,128)(2,1)}, u32[]{:S(2)}, u32[]{:S(2)}) collective-permute-start(bf16[4,160,256]{2,1,0:T(8,128)(2,1)} %shard_map.196.refs_0_), channel_id=1, source_target_pairs={{0,32},{32,64},{64,96},{96,128},{128,160},{160,192},{192,224},{224... | collective-permute-start | bytes 983048 | tf_op jit(solution)/shard_map/ppermute | solution.py:408
  49.8 18.5 %collective-permute-start.28 = (bf16[256,1024]{1,0:T(8,128)(2,1)S(1)}, bf16[256,1024]{1,0:T(8,128)(2,1)S(1)}, u32[]{:S(2)}, u32[]{:S(2)}) collective-permute-start(bf16[256,1024]{1,0:T(8,128)(2,1)S(1)} %get-tuple-element.22), channel_id=1, source_target_pairs={{0,3},{1,2},{2,1},{3,0},{4,7},{5,6},{6,5},{7,4},{8,11},{9,10},{10,... | collective-permute-start | bytes 1572872 | tf_op jit(solution)/shard_map/ppermute | solution.py:387
  53.0 22.9 %collective-permute-start.21 = (bf16[256,1024]{1,0:T(8,128)(2,1)S(1)}, bf16[256,1024]{1,0:T(8,128)(2,1)S(1)}, u32[]{:S(2)}, u32[]{:S(2)}) collective-permute-start(bf16[256,1024]{1,0:T(8,128)(2,1)S(1)} %get-tuple-element.23), channel_id=1, source_target_pairs={{0,3},{1,2},{2,1},{3,0},{4,7},{5,6},{6,5},{7,4},{8,11},{9,10},{10,... | collective-permute-start | bytes 1572872 | tf_op jit(solution)/shard_map/ppermute | solution.py:387
  55.7 25.1 %collective-permute-start.6 = (bf16[4,160,256]{2,1,0:T(8,128)(2,1)}, bf16[4,160,256]{2,1,0:T(8,128)(2,1)}, u32[]{:S(2)}, u32[]{:S(2)}) collective-permute-start(bf16[4,160,256]{2,1,0:T(8,128)(2,1)} %shard_map.196.refs_0_), channel_id=1, source_target_pairs={{0,224},{32,0},{64,32},{96,64},{128,96},{160,128},{192,160},{224,1... | collective-permute-start | bytes 983048 | tf_op jit(solution)/shard_map/ppermute | solution.py:411
  56.8 24.1 %collective-permute-start.25 = (bf16[256,1024]{1,0:T(8,128)(2,1)S(1)}, bf16[256,1024]{1,0:T(8,128)(2,1)S(1)}, u32[]{:S(2)}, u32[]{:S(2)}) collective-permute-start(bf16[256,1024]{1,0:T(8,128)(2,1)S(1)} %copy-done.3), channel_id=1, source_target_pairs={{0,1},{1,0},{2,3},{3,2},{4,5},{5,4},{6,7},{7,6},{8,9},{9,8},{10,11... | collective-permute-start | bytes 1572872 | tf_op jit(solution)/shard_map/ppermute | solution.py:359
  67.0 22.4 %collective-permute-start.27 = (bf16[256,1024]{1,0:T(8,128)(2,1)}, bf16[256,1024]{1,0:T(8,128)(2,1)S(1)}, u32[]{:S(2)}, u32[]{:S(2)}) collective-permute-start(bf16[256,1024]{1,0:T(8,128)(2,1)} %collective-permute-done.26.w2_ref), channel_id=1, source_target_pairs={{0,1},{1,0},{2,3},{3,2},{4,5},{5,4},{6,7},{7,6},{8,9},{9,8},{10,11... | collective-permute-start | bytes 1572872 | tf_op jit(solution)/shard_map/ppermute | solution.py:360
  68.3 13.6 %collective-permute-start.8 = (bf16[4,160,256]{2,1,0:T(8,128)(2,1)}, bf16[4,160,256]{2,1,0:T(8,128)(2,1)}, u32[]{:S(2)}, u32[]{:S(2)}) collective-permute-start(bf16[4,160,256]{2,1,0:T(8,128)(2,1)} %collective-permute-done.4.refs_2_), channel_id=1, source_target_pairs={{0,32},{32,64},{64,96},{96,128},{128,160},{160,192},{192,224},{224... | collective-permute-start | bytes 983048 | tf_op jit(solution)/shard_map/ppermute | solution.py:408
  75.8 13.5 %collective-permute-start.29 = (bf16[256,512]{1,0:T(8,128)(2,1)S(1)}, bf16[256,512]{1,0:T(8,128)(2,1)S(1)}, u32[]{:S(2)}, u32[]{:S(2)}) collective-permute-start(bf16[256,512]{1,0:T(8,128)(2,1)S(1)} %shard_map.200.a_ref), channel_id=1, source_target_pairs={{0,3},{1,2},{2,1},{3,0},{4,7},{5,6},{6,5},{7,4},{8,11},{9,10},{10,... | collective-permute-start | bytes 786440 | tf_op jit(solution)/shard_map/ppermute | solution.py:394
  80.8 10.3 %collective-permute-start.24 = (bf16[256,512]{1,0:T(8,128)(2,1)S(1)}, bf16[256,512]{1,0:T(8,128)(2,1)S(1)}, u32[]{:S(2)}, u32[]{:S(2)}) collective-permute-start(bf16[256,512]{1,0:T(8,128)(2,1)S(1)} %shard_map.198.a_ref), channel_id=1, source_target_pairs={{0,3},{1,2},{2,1},{3,0},{4,7},{5,6},{6,5},{7,4},{8,11},{9,10},{10,... | collective-permute-start | bytes 786440 | tf_op jit(solution)/shard_map/ppermute | solution.py:394
  80.9 27.7 %collective-permute-start.10 = (bf16[4,160,256]{2,1,0:T(8,128)(2,1)}, bf16[4,160,256]{2,1,0:T(8,128)(2,1)S(1)}, u32[]{:S(2)}, u32[]{:S(2)}) collective-permute-start(bf16[4,160,256]{2,1,0:T(8,128)(2,1)} %collective-permute-done.6.refs_4_), channel_id=1, source_target_pairs={{0,224},{32,0},{64,32},{96,64},{128,96},{160,128},{192,160},{224,1... | collective-permute-start | bytes 983048 | tf_op jit(solution)/shard_map/ppermute | solution.py:411
  81.8 29.5 %collective-permute-start.12 = (bf16[4,160,256]{2,1,0:T(8,128)(2,1)}, bf16[4,160,256]{2,1,0:T(8,128)(2,1)S(1)}, u32[]{:S(2)}, u32[]{:S(2)}) collective-permute-start(bf16[4,160,256]{2,1,0:T(8,128)(2,1)} %collective-permute-done.8.refs_6_), channel_id=1, source_target_pairs={{0,32},{32,64},{64,96},{96,128},{128,160},{160,192},{192,224},{224... | collective-permute-start | bytes 983048 | tf_op jit(solution)/shard_map/ppermute | solution.py:408
  94.0 75.1 %all-to-all-start.1 = ((bf16[128,8,512]{2,1,0:T(8,128)(2,1)}), bf16[128,8,512]{2,1,0:T(8,128)(2,1)S(1)}, u32[]{:S(2)}, u32[]{:S(2)}) async-start(bf16[128,8,512]{2,1,0:T(8,128)(2,1)} %bitcast.12), calls=%async_computation.1 | async-start | bytes 2097152 | tf_op jit(solution)/shard_map/all_to_all | solution.py:439
  107.1 4.2 %collective-permute-start.3 = (bf16[4,160,256]{2,1,0:T(8,128)(2,1)}, bf16[4,160,256]{2,1,0:T(8,128)(2,1)S(1)}, u32[]{:S(2)}, u32[]{:S(2)}) collective-permute-start(bf16[4,160,256]{2,1,0:T(8,128)(2,1)} %shard_map.196.refs_0_), channel_id=1, source_target_pairs={{0,4},{4,0},{1,5},{5,1},{2,6},{6,2},{3,7},{7,3},{8,12},{12,8},{9,1... | collective-permute-start | bytes 983048 | tf_op jit(solution)/shard_map/ppermute | solution.py:415
  108.1 3.7 %collective-permute-start.5 = (bf16[4,160,256]{2,1,0:T(8,128)(2,1)}, bf16[4,160,256]{2,1,0:T(8,128)(2,1)S(1)}, u32[]{:S(2)}, u32[]{:S(2)}) collective-permute-start(bf16[4,160,256]{2,1,0:T(8,128)(2,1)} %collective-permute-done.4.refs_2_), channel_id=1, source_target_pairs={{0,4},{4,0},{1,5},{5,1},{2,6},{6,2},{3,7},{7,3},{8,12},{12,8},{9,1... | collective-permute-start | bytes 983048 | tf_op jit(solution)/shard_map/ppermute | solution.py:415
  108.2 4.0 %collective-permute-start.7 = (bf16[4,160,256]{2,1,0:T(8,128)(2,1)}, bf16[4,160,256]{2,1,0:T(8,128)(2,1)S(1)}, u32[]{:S(2)}, u32[]{:S(2)}) collective-permute-start(bf16[4,160,256]{2,1,0:T(8,128)(2,1)} %collective-permute-done.6.refs_4_), channel_id=1, source_target_pairs={{0,4},{4,0},{1,5},{5,1},{2,6},{6,2},{3,7},{7,3},{8,12},{12,8},{9,1... | collective-permute-start | bytes 983048 | tf_op jit(solution)/shard_map/ppermute | solution.py:415
  108.6 29.4 %collective-permute-start.14 = (bf16[4,160,256]{2,1,0:T(8,128)(2,1)S(1)}, bf16[4,160,256]{2,1,0:T(8,128)(2,1)S(1)}, u32[]{:S(2)}, u32[]{:S(2)}) collective-permute-start(bf16[4,160,256]{2,1,0:T(8,128)(2,1)S(1)} %collective-permute-done.10.refs_8_), channel_id=1, source_target_pairs={{0,224},{32,0},{64,32},{96,64},{128,96},{160,128},{192,160},{224,1... | collective-permute-start | bytes 983048 | tf_op jit(solution)/shard_map/ppermute | solution.py:411
  111.3 28.5 %collective-permute-start.16 = (bf16[4,160,256]{2,1,0:T(8,128)(2,1)S(1)}, bf16[4,160,256]{2,1,0:T(8,128)(2,1)S(1)}, u32[]{:S(2)}, u32[]{:S(2)}) collective-permute-start(bf16[4,160,256]{2,1,0:T(8,128)(2,1)S(1)} %collective-permute-done.12.refs_10_), channel_id=1, source_target_pairs={{0,32},{32,64},{64,96},{96,128},{128,160},{160,192},{192,224},{224... | collective-permute-start | bytes 983048 | tf_op jit(solution)/shard_map/ppermute | solution.py:408
  111.3 29.9 %collective-permute-start.11 = (bf16[4,160,256]{2,1,0:T(8,128)(2,1)S(1)}, bf16[4,160,256]{2,1,0:T(8,128)(2,1)S(1)}, u32[]{:S(2)}, u32[]{:S(2)}) collective-permute-start(bf16[4,160,256]{2,1,0:T(8,128)(2,1)S(1)} %collective-permute-done.10.refs_8_), channel_id=1, source_target_pairs={{0,4},{4,0},{1,5},{5,1},{2,6},{6,2},{3,7},{7,3},{8,12},{12,8},{9,1... | collective-permute-start | bytes 983048 | tf_op jit(solution)/shard_map/ppermute | solution.py:415
  111.8 29.5 %collective-permute-start.9 = (bf16[4,160,256]{2,1,0:T(8,128)(2,1)}, bf16[4,160,256]{2,1,0:T(8,128)(2,1)S(1)}, u32[]{:S(2)}, u32[]{:S(2)}) collective-permute-start(bf16[4,160,256]{2,1,0:T(8,128)(2,1)} %collective-permute-done.8.refs_6_), channel_id=1, source_target_pairs={{0,4},{4,0},{1,5},{5,1},{2,6},{6,2},{3,7},{7,3},{8,12},{12,8},{9,1... | collective-permute-start | bytes 983048 | tf_op jit(solution)/shard_map/ppermute | solution.py:415
  112.2 29.1 %collective-permute-start.13 = (bf16[4,160,256]{2,1,0:T(8,128)(2,1)S(1)}, bf16[4,160,256]{2,1,0:T(8,128)(2,1)S(1)}, u32[]{:S(2)}, u32[]{:S(2)}) collective-permute-start(bf16[4,160,256]{2,1,0:T(8,128)(2,1)S(1)} %collective-permute-done.12.refs_10_), channel_id=1, source_target_pairs={{0,4},{4,0},{1,5},{5,1},{2,6},{6,2},{3,7},{7,3},{8,12},{12,8},{9,1... | collective-permute-start | bytes 983048 | tf_op jit(solution)/shard_map/ppermute | solution.py:415
  138.0 3.3 %collective-permute-start.15 = (bf16[4,160,256]{2,1,0:T(8,128)(2,1)S(1)}, bf16[4,160,256]{2,1,0:T(8,128)(2,1)S(1)}, u32[]{:S(2)}, u32[]{:S(2)}) collective-permute-start(bf16[4,160,256]{2,1,0:T(8,128)(2,1)S(1)} %collective-permute-done.14.refs_12_), channel_id=1, source_target_pairs={{0,4},{4,0},{1,5},{5,1},{2,6},{6,2},{3,7},{7,3},{8,12},{12,8},{9,1... | collective-permute-start | bytes 983048 | tf_op jit(solution)/shard_map/ppermute | solution.py:415
  139.9 2.2 %collective-permute-start.17 = (bf16[4,160,256]{2,1,0:T(8,128)(2,1)S(1)}, bf16[4,160,256]{2,1,0:T(8,128)(2,1)S(1)}, u32[]{:S(2)}, u32[]{:S(2)}) collective-permute-start(bf16[4,160,256]{2,1,0:T(8,128)(2,1)S(1)} %collective-permute-done.16.refs_14_), channel_id=1, source_target_pairs={{0,4},{4,0},{1,5},{5,1},{2,6},{6,2},{3,7},{7,3},{8,12},{12,8},{9,1... | collective-permute-start | bytes 983048 | tf_op jit(solution)/shard_map/ppermute | solution.py:415
  158.5 6.0 %collective-permute-start.18 = (bf16[32,2048]{1,0:T(8,128)(2,1)S(1)}, bf16[32,2048]{1,0:T(8,128)(2,1)S(1)}, u32[]{:S(2)}, u32[]{:S(2)}) collective-permute-start(bf16[32,2048]{1,0:T(8,128)(2,1)S(1)} %get-tuple-element.13), channel_id=1, source_target_pairs={{0,1},{1,2},{2,3},{3,0},{4,5},{5,6},{6,7},{7,4},{8,9},{9,10},{10,1... | collective-permute-start | bytes 393224 | tf_op jit(solution)/shard_map/ppermute | solution.py:436
  159.8 8.6 %collective-permute-start.19 = (bf16[32,2048]{1,0:T(8,128)(2,1)S(1)}, bf16[32,2048]{1,0:T(8,128)(2,1)S(1)}, u32[]{:S(2)}, u32[]{:S(2)}) collective-permute-start(bf16[32,2048]{1,0:T(8,128)(2,1)S(1)} %get-tuple-element.14), channel_id=1, source_target_pairs={{0,2},{1,3},{2,0},{3,1},{4,6},{5,7},{6,4},{7,5},{8,10},{9,11},{10,... | collective-permute-start | bytes 393224 | tf_op jit(solution)/shard_map/ppermute | solution.py:436
  162.4 6.0 %collective-permute-start.20 = (bf16[32,2048]{1,0:T(8,128)(2,1)S(1)}, bf16[32,2048]{1,0:T(8,128)(2,1)S(1)}, u32[]{:S(2)}, u32[]{:S(2)}) collective-permute-start(bf16[32,2048]{1,0:T(8,128)(2,1)S(1)} %get-tuple-element.15), channel_id=1, source_target_pairs={{0,3},{1,0},{2,1},{3,2},{4,7},{5,4},{6,5},{7,6},{8,11},{9,8},{10,9... | collective-permute-start | bytes 393224 | tf_op jit(solution)/shard_map/ppermute | solution.py:436
  (21 other events, 447.2 us)
where the time goes:
time: 172 us; the launch traced here: 171 us
  waiting for transfers between devices  65.1 us (38%)
  starting transfers between devices  63.2 us (37%)
  Pallas kernels  35.1 us (20%)
  local copies, waits for them, and re-layouts  5.7 us (3%)
    ppermute x3, waiting for transfers between devices, inner(): low = lax.ppermute(low, 'z', ahead(depth - 1, depth))  25.6 us
    pallas_call x1, Pallas kernels, inner(): pl.pallas_call(functools.partial(attend_kernel, count), out_shape=[share]...  16.4 us
    pallas_call x10, Pallas kernels, call(): pl.pallas_call(kernel, out_shape=out_shape, in_specs=[smem() if a.size ==...  16.3 us
    all_to_all x1, waiting for transfers between devices, inner(): arrived = lax.all_to_all(outgoing, EP, 0, 0, tiled=True)  14.6 us
    all_to_all x1, starting transfers between devices, inner(): lax.all_to_all(result.reshape(2 * experts, per, part // 2), (*EP, 'yl'),...  13.1 us
    all_to_all x1, starting transfers between devices, inner(): arrived = lax.all_to_all(outgoing, EP, 0, 0, tiled=True)  13 us
    ppermute x1, waiting for transfers between devices, inner(): far_up = lax.ppermute(w_up[0], TP, across(1))  10.1 us
    ppermute x1, waiting for transfers between devices, inner(): down2 = lax.ppermute(down3, TP, across(1))  6.9 us
  transfers between devices with their start and end apart: 32, of which 10 were waited for; matrix products, arithmetic and copies ran while one was open for 1% of the time, Pallas kernels for 18%

commit v1 on v0

--- a/solution.py
+++ b/solution.py
@@ -102,10 +102,11 @@
     blocks = kv_ref.shape[1]
     ways = rank // ROPE
     few = tok_rows // ways
+    group = 4
 
     def step(j, carry):
         latent, turned = [], []
-        for i in (2 * j, 2 * j + 1):
+        for i in (group * j + k for k in range(group)):
             pltpu.make_async_copy(kv_ref.at[i], kv_ref.at[i], sem.at[i]).wait()
             for q in range(ways):
                 latent.append(kv_ref[i, :, q * few : (q + 1) * few, :].reshape(blocks * few, rank))
@@ -128,7 +129,7 @@
             acc_ref[h] = acc_ref[h] * shrink + added
         return carry
 
-    lax.fori_loop(0, count // 2, step, 0)
+    lax.fori_loop(0, count // group, step, 0)
     parts = [(acc_ref[h] / l_ref[h : h + 1, :]).astype(bf16) for h in range(heads)]
     all_ref[...] = dot_0(jnp.concatenate(parts, axis=0), wo_ref[...]).astype(bf16)
     share = tok_rows // len(out_refs)
@@ -350,7 +351,12 @@
         compiler_params=params(48),
         cost_estimate=pl.CostEstimate(flops=6 * 10**8, transcendentals=0, bytes_accessed=4 * 10**6),
         name="prep",
-    )(me, tokens_b, ffn_gain.reshape(1, -1), route_expert.T)
+    )(
+        me,
+        pltpu.with_memory_space_constraint(tokens_b, pltpu.HBM),
+        pltpu.with_memory_space_constraint(ffn_gain.reshape(1, -1), pltpu.HBM),
+        pltpu.with_memory_space_constraint(route_expert.T, pltpu.HBM),
+    )
     arrived = lax.all_to_all(outgoing, EP, 0, 0, tiled=True)
     arrived = arrived.reshape(rows, part)
 
@@ -411,7 +417,7 @@
             low = lax.ppermute(low, "z", ahead(depth - 1, depth))
             near.append(low)
     pieces = []
-    for piece in near[:depth]:
+    for piece in near:
         pieces += [piece, lax.ppermute(piece, "c", [(0, 1), (1, 0)])]
 
     share = shape(tok_a // tp, w_out.shape[1])

time: 172 us -> 168 us (0.977)
  local copies, waits for them, and re-layouts: 5.7 us -> 2.74 us
    unnamed x44 -> x38, local copies, waits for them, and re-layouts: 5.49 us -> 2.53 us
  transfers between devices with their start and end apart: 32 -> 32, of which waited for: 10 -> 10; matrix products, arithmetic and copies ran while one was open for 1% -> 1% of each run, Pallas kernels for 18% -> 17%
where the time goes in v1:
time: 168 us
  waiting for transfers between devices  65.2 us (39%)
  starting transfers between devices  63.2 us (38%)
  Pallas kernels  34.3 us (20%)
  local copies, waits for them, and re-layouts  2.74 us (2%)
    ppermute x3, waiting for transfers between devices, inner(): low = lax.ppermute(low, 'z', ahead(depth - 1, depth))  25.6 us
    pallas_call x10, Pallas kernels, call(): pl.pallas_call(kernel, out_shape=out_shape, in_specs=[smem() if a.size ==...  16.3 us
    pallas_call x1, Pallas kernels, inner(): pl.pallas_call(functools.partial(attend_kernel, count), out_shape=[share]...  14.9 us
    all_to_all x1, waiting for transfers between devices, inner(): arrived = lax.all_to_all(outgoing, EP, 0, 0, tiled=True)  14.6 us
    all_to_all x1, starting transfers between devices, inner(): lax.all_to_all(result.reshape(2 * experts, per, part // 2), (*EP, 'yl'),...  13.2 us
    all_to_all x1, starting transfers between devices, inner(): arrived = lax.all_to_all(outgoing, EP, 0, 0, tiled=True)  13 us
    ppermute x1, waiting for transfers between devices, inner(): far_up = lax.ppermute(w_up[0], TP, across(1))  10.1 us
    ppermute x1, waiting for transfers between devices, inner(): down2 = lax.ppermute(down3, TP, across(1))  6.88 us
  transfers between devices with their start and end apart: 32, of which 10 were waited for; matrix products, arithmetic and copies ran while one was open for 1% of the time, Pallas kernels for 17%

profile of v1, /device:TPU:1, one launch (start us, length us, event | category | flops | bytes accessed | tf_op | source)
XLA Modules:
  0.0 167.5 jit_solution(13801841281376575874)
XLA Ops:
  0.7 3.1 %prep.1 = (s32[2,512]{1,0:T(2,128)S(1)}, bf16[64,8,1024]{2,1,0:T(8,128)(2,1)S(1)}) custom-call(s32[1]{0:T(128)} %bitcast.me_ref, bf16[512,2048]{1,0:T(8,128)(2,1)} %tok_hbm.1, f32[1,2048]{1,0:T(1,128)} %bitcast.30, s32[2,512]{1,0:T(2,128)} %bitcast.31), custom_call_target="tpu_custom_call" | custom-call | flops 600000000 | bytes 4000000 | tf_op jit(solution)/shard_map/prep/pallas_call | solution.py:337
  4.8 13.0 %all-to-all-start = ((bf16[64,8,1024]{2,1,0:T(8,128)(2,1)}), bf16[64,8,1024]{2,1,0:T(8,128)(2,1)S(1)}, u32[]{:S(2)}, u32[]{:S(2)}) async-start(bf16[64,8,1024]{2,1,0:T(8,128)(2,1)} %copy-done.5), calls=%async_computation | async-start | bytes 2097152 | tf_op jit(solution)/shard_map/all_to_all | solution.py:360
  17.8 1.4 collective-permute-start.22
  20.1 1.4 collective-permute-start
  21.4 2.4 %collective-permute-start.1 = (bf16[160,256]{1,0:T(8,128)(2,1)S(1)}, bf16[160,256]{1,0:T(8,128)(2,1)S(1)}, u32[]{:S(2)}, u32[]{:S(2)}) collective-permute-start(bf16[160,256]{1,0:T(8,128)(2,1)S(1)} %shard_map.195.refs_0_), channel_id=1, source_target_pairs={{0,16},{8,24},{16,0},{24,8},{1,17},{9,25},{17,1},{25,9},{2,18},{10... | collective-permute-start | bytes 245768 | tf_op jit(solution)/shard_map/ppermute | solution.py:379
  23.8 1.2 collective-permute-start.2
  25.0 1.2 copy-done.4
  27.1 2.7 %collective-permute-start.26 = (bf16[256,1024]{1,0:T(8,128)(2,1)}, bf16[256,1024]{1,0:T(8,128)(2,1)}, u32[]{:S(2)}, u32[]{:S(2)}) collective-permute-start(bf16[256,1024]{1,0:T(8,128)(2,1)} %get-tuple-element.20), channel_id=1, source_target_pairs={{0,3},{1,2},{2,1},{3,0},{4,7},{5,6},{6,5},{7,4},{8,11},{9,10},{10,... | collective-permute-start | bytes 1572872 | tf_op jit(solution)/shard_map/ppermute | solution.py:364
  30.6 2.2 %collective-permute-start.4 = (bf16[4,160,256]{2,1,0:T(8,128)(2,1)}, bf16[4,160,256]{2,1,0:T(8,128)(2,1)}, u32[]{:S(2)}, u32[]{:S(2)}) collective-permute-start(bf16[4,160,256]{2,1,0:T(8,128)(2,1)} %shard_map.196.refs_0_), channel_id=1, source_target_pairs={{0,32},{32,64},{64,96},{96,128},{128,160},{160,192},{192,224},{224... | collective-permute-start | bytes 983048 | tf_op jit(solution)/shard_map/ppermute | solution.py:414
  32.9 14.6 %all-to-all-done = bf16[64,8,1024]{2,1,0:T(8,128)(2,1)S(1)} async-done(((bf16[64,8,1024]{2,1,0:T(8,128)(2,1)}), bf16[64,8,1024]{2,1,0:T(8,128)(2,1)S(1)}, u32[]{:S(2)}, u32[]{:S(2)}) %all-to-all-start) | async-done | bytes 1048608 | tf_op jit(solution)/shard_map/all_to_all | solution.py:360
  47.5 2.8 %collective-permute-start.28 = (bf16[256,1024]{1,0:T(8,128)(2,1)S(1)}, bf16[256,1024]{1,0:T(8,128)(2,1)S(1)}, u32[]{:S(2)}, u32[]{:S(2)}) collective-permute-start(bf16[256,1024]{1,0:T(8,128)(2,1)S(1)} %get-tuple-element.22), channel_id=1, source_target_pairs={{0,3},{1,2},{2,1},{3,0},{4,7},{5,6},{6,5},{7,4},{8,11},{9,10},{10,... | collective-permute-start | bytes 1572872 | tf_op jit(solution)/shard_map/ppermute | solution.py:393
  50.7 2.7 %collective-permute-start.21 = (bf16[256,1024]{1,0:T(8,128)(2,1)S(1)}, bf16[256,1024]{1,0:T(8,128)(2,1)S(1)}, u32[]{:S(2)}, u32[]{:S(2)}) collective-permute-start(bf16[256,1024]{1,0:T(8,128)(2,1)S(1)} %get-tuple-element.23), channel_id=1, source_target_pairs={{0,3},{1,2},{2,1},{3,0},{4,7},{5,6},{6,5},{7,4},{8,11},{9,10},{10,... | collective-permute-start | bytes 1572872 | tf_op jit(solution)/shard_map/ppermute | solution.py:393
  53.5 1.1 collective-permute-start.6
  54.6 10.1 %collective-permute-done.23.vu_ref = bf16[2048,256]{1,0:T(8,128)(2,1)} collective-permute-done((bf16[2048,256]{1,0:T(8,128)(2,1)S(1)}, bf16[2048,256]{1,0:T(8,128)(2,1)}, u32[]{:S(2)}, u32[]{:S(2)}) %collective-permute-start.23) | collective-permute-done | bytes 1048608 | tf_op jit(solution)/shard_map/ppermute | solution.py:329
  64.7 1.3 collective-permute-start.27
  66.0 1.4 collective-permute-start.8
  67.4 2.8 %shard_map.197 = (f32[256,1024]{1,0:T(8,128)S(1)}, f32[256,1024]{1,0:T(8,128)S(1)}) custom-call(s32[1]{0:T(128)} %bitcast.me_ref, bf16[512,1024]{1,0:T(8,128)(2,1)S(1)} %bitcast.16, bf16[2048,256]{1,0:T(8,128)(2,1)S(1)} %bitcast.18, bf16[2048,256]{1,0:T(8,128)(2,1)S(1)} %bitcast.22, bf16[2048,256]{1,0:T(8,128)(2,1)} %collective-permute-done.22.vg_ref, ...), custom_call_target="tpu_custom_call" | custom-call | flops 1073741824 | bytes 7340036 | tf_op jit(solution)/shard_map/pallas_call | solution.py:284
  70.2 2.3 %shard_map.200.a_ref = bf16[256,512]{1,0:T(8,128)(2,1)S(1)} custom-call(s32[1]{0:T(128)} %bitcast.me_ref, bf16[256,1024]{1,0:T(8,128)(2,1)S(1)} %collective-permute-done.28.b_ref, bf16[2048,256]{1,0:T(8,128)(2,1)S(1)} %bitcast.19, bf16[2048,256]{1,0:T(8,128)(2,1)S(1)} %bitcast.23, bf16[2048,256]{1,0:T(8,128)(2,1)} %collective-permute-done.22.vg_ref, ...), custom_call_target="tpu_custom_call" | custom-call | flops 536870912 | bytes 6029316 | tf_op jit(solution)/shard_map/pallas_call | solution.py:284
  72.5 1.1 collective-permute-done.21.b_ref
  73.6 2.6 %collective-permute-start.29 = (bf16[256,512]{1,0:T(8,128)(2,1)S(1)}, bf16[256,512]{1,0:T(8,128)(2,1)S(1)}, u32[]{:S(2)}, u32[]{:S(2)}) collective-permute-start(bf16[256,512]{1,0:T(8,128)(2,1)S(1)} %shard_map.200.a_ref), channel_id=1, source_target_pairs={{0,3},{1,2},{2,1},{3,0},{4,7},{5,6},{6,5},{7,4},{8,11},{9,10},{10,... | collective-permute-start | bytes 786440 | tf_op jit(solution)/shard_map/ppermute | solution.py:400
  76.2 2.3 %shard_map.198.a_ref = bf16[256,512]{1,0:T(8,128)(2,1)S(1)} custom-call(s32[1]{0:T(128)} %bitcast.me_ref, bf16[256,1024]{1,0:T(8,128)(2,1)S(1)} %collective-permute-done.21.b_ref, bf16[2048,256]{1,0:T(8,128)(2,1)S(1)} %bitcast.20, bf16[2048,256]{1,0:T(8,128)(2,1)S(1)} %bitcast.24, bf16[2048,256]{1,0:T(8,128)(2,1)} %collective-permute-done.22.vg_ref, ...), custom_call_target="tpu_custom_call" | custom-call | flops 536870912 | bytes 6029316 | tf_op jit(solution)/shard_map/pallas_call | solution.py:284
  80.2 6.9 %collective-permute-done.27.w3_ref = bf16[256,1024]{1,0:T(8,128)(2,1)S(1)} collective-permute-done((bf16[256,1024]{1,0:T(8,128)(2,1)}, bf16[256,1024]{1,0:T(8,128)(2,1)S(1)}, u32[]{:S(2)}, u32[]{:S(2)}) %collective-permute-start.27) | collective-permute-done | bytes 524320 | tf_op jit(solution)/shard_map/ppermute | solution.py:366
  87.1 1.8 %shard_map.201.rest_0_ = bf16[32,2,8,512]{3,2,1,0:T(8,128)(2,1)S(1)} custom-call(bf16[256,512]{1,0:T(8,128)(2,1)S(1)} %shard_map.200.a_ref, bf16[256,512]{1,0:T(8,128)(2,1)S(1)} %collective-permute-done.29.b_ref, bf16[256,1024]{1,0:T(8,128)(2,1)S(1)} %copy-done.3, bf16[256,1024]{1,0:T(8,128)(2,1)S(1)} %collective-permute-done.25.w1_ref, ...), custom_call_target="tpu_custom_call" | custom-call | flops 536870912 | bytes 3145728 | tf_op jit(solution)/shard_map/pallas_call | solution.py:284
  88.9 2.8 %shard_map.202 = bf16[64,2,8,512]{3,2,1,0:T(8,128)(2,1)} custom-call(bf16[256,512]{1,0:T(8,128)(2,1)S(1)} %shard_map.198.a_ref, bf16[256,512]{1,0:T(8,128)(2,1)S(1)} %collective-permute-done.24.b_ref, bf16[256,1024]{1,0:T(8,128)(2,1)S(1)} %copy-done.3, bf16[256,1024]{1,0:T(8,128)(2,1)S(1)} %collective-permute-done.25.w1_ref, ...), custom_call_target="tpu_custom_call" | custom-call | flops 536870912 | bytes 4194304 | tf_op jit(solution)/shard_map/pallas_call | solution.py:284
  91.7 13.2 %all-to-all-start.1 = ((bf16[128,8,512]{2,1,0:T(8,128)(2,1)}), bf16[128,8,512]{2,1,0:T(8,128)(2,1)S(1)}, u32[]{:S(2)}, u32[]{:S(2)}) async-start(bf16[128,8,512]{2,1,0:T(8,128)(2,1)} %bitcast.12), calls=%async_computation.1 | async-start | bytes 2097152 | tf_op jit(solution)/shard_map/all_to_all | solution.py:445
  106.4 2.7 %collective-permute-start.14 = (bf16[4,160,256]{2,1,0:T(8,128)(2,1)S(1)}, bf16[4,160,256]{2,1,0:T(8,128)(2,1)S(1)}, u32[]{:S(2)}, u32[]{:S(2)}) collective-permute-start(bf16[4,160,256]{2,1,0:T(8,128)(2,1)S(1)} %collective-permute-done.10.refs_8_), channel_id=1, source_target_pairs={{0,224},{32,0},{64,32},{96,64},{128,96},{160,128},{192,160},{224,1... | collective-permute-start | bytes 983048 | tf_op jit(solution)/shard_map/ppermute | solution.py:417
  110.1 25.6 %collective-permute-done.14.refs_12_ = bf16[4,160,256]{2,1,0:T(8,128)(2,1)S(1)} collective-permute-done((bf16[4,160,256]{2,1,0:T(8,128)(2,1)S(1)}, bf16[4,160,256]{2,1,0:T(8,128)(2,1)S(1)}, u32[]{:S(2)}, u32[]{:S(2)}) %collective-permute-start.14) | collective-permute-done | bytes 327712 | tf_op jit(solution)/shard_map/ppermute | solution.py:417
  139.8 14.9 %attend.1 = (bf16[32,2048]{1,0:T(8,128)(2,1)S(1)}, bf16[32,2048]{1,0:T(8,128)(2,1)S(1)}, bf16[32,2048]{1,0:T(8,128)(2,1)S(1)}, bf16[32,2048]{1,0:T(8,128)(2,1)S(1)}) custom-call(s32[1]{0:T(128)} %bitcast.me_ref, bf16[2,128,256]{2,1,0:T(8,128)(2,1)S(1)} %shard_map.194.q_ref, bf16[256,256]{1,0:T(8,128)(2,1)S(1)} %copy-done.12, ...), custom_call_target="tpu_custom_call" | custom-call | flops 6000000000 | bytes 8000000 | tf_op jit(solution)/shard_map/attend/pallas_call | solution.py:425
  154.8 1.3 collective-permute-start.18
  156.0 2.6 %collective-permute-start.19 = (bf16[32,2048]{1,0:T(8,128)(2,1)S(1)}, bf16[32,2048]{1,0:T(8,128)(2,1)S(1)}, u32[]{:S(2)}, u32[]{:S(2)}) collective-permute-start(bf16[32,2048]{1,0:T(8,128)(2,1)S(1)} %get-tuple-element.14), channel_id=1, source_target_pairs={{0,2},{1,3},{2,0},{3,1},{4,6},{5,7},{6,4},{7,5},{8,10},{9,11},{10,... | collective-permute-start | bytes 393224 | tf_op jit(solution)/shard_map/ppermute | solution.py:442
  160.7 4.0 %collective-permute-done.19 = bf16[32,2048]{1,0:T(8,128)(2,1)S(1)} collective-permute-done((bf16[32,2048]{1,0:T(8,128)(2,1)S(1)}, bf16[32,2048]{1,0:T(8,128)(2,1)S(1)}, u32[]{:S(2)}, u32[]{:S(2)}) %collective-permute-start.19) | collective-permute-done | bytes 131104 | tf_op jit(solution)/shard_map/ppermute | solution.py:442
  165.4 2.1 %shard_map.203 = bf16[512,512]{1,0:T(8,128)(2,1)} custom-call(s32[512,2]{1,0:T(8,128)S(1)} %bitcast.27, f32[512,2]{1,0:T(8,128)S(1)} %copy.23.weight_ref, bf16[1024,512]{1,0:T(8,128)(2,1)S(1)} %bitcast.26), custom_call_target="tpu_custom_call" | custom-call | flops 1073741824 | bytes 1581056 | tf_op jit(solution)/shard_map/pallas_call | solution.py:284
  (87 shorter events, 14.9 us)
Async XLA Ops:
  4.8 42.6 %all-to-all-start = ((bf16[64,8,1024]{2,1,0:T(8,128)(2,1)}), bf16[64,8,1024]{2,1,0:T(8,128)(2,1)S(1)}, u32[]{:S(2)}, u32[]{:S(2)}) async-start(bf16[64,8,1024]{2,1,0:T(8,128)(2,1)} %copy-done.5), calls=%async_computation | async-start | bytes 2097152 | tf_op jit(solution)/shard_map/all_to_all | solution.py:360
  17.8 36.8 %collective-permute-start.22 = (bf16[2048,256]{1,0:T(8,128)(2,1)S(1)}, bf16[2048,256]{1,0:T(8,128)(2,1)}, u32[]{:S(2)}, u32[]{:S(2)}) collective-permute-start(bf16[2048,256]{1,0:T(8,128)(2,1)S(1)} %bitcast.17), channel_id=1, source_target_pairs={{0,1},{1,0},{2,3},{3,2},{4,5},{5,4},{6,7},{7,6},{8,9},{9,8},{10,11... | collective-permute-start | bytes 3145736 | tf_op jit(solution)/shard_map/ppermute | solution.py:328
  19.2 45.5 %collective-permute-start.23 = (bf16[2048,256]{1,0:T(8,128)(2,1)S(1)}, bf16[2048,256]{1,0:T(8,128)(2,1)}, u32[]{:S(2)}, u32[]{:S(2)}) collective-permute-start(bf16[2048,256]{1,0:T(8,128)(2,1)S(1)} %bitcast.21), channel_id=1, source_target_pairs={{0,1},{1,0},{2,3},{3,2},{4,5},{5,4},{6,7},{7,6},{8,9},{9,8},{10,11... | collective-permute-start | bytes 3145736 | tf_op jit(solution)/shard_map/ppermute | solution.py:329
  20.1 7.0 %collective-permute-start = (bf16[160,256]{1,0:T(8,128)(2,1)S(1)}, bf16[160,256]{1,0:T(8,128)(2,1)S(1)}, u32[]{:S(2)}, u32[]{:S(2)}) collective-permute-start(bf16[160,256]{1,0:T(8,128)(2,1)S(1)} %shard_map.195.refs_0_), channel_id=1, source_target_pairs={{0,8},{8,16},{16,24},{24,0},{1,9},{9,17},{17,25},{25,1},{2,10},{10... | collective-permute-start | bytes 245768 | tf_op jit(solution)/shard_map/ppermute | solution.py:379
  21.4 8.4 %collective-permute-start.1 = (bf16[160,256]{1,0:T(8,128)(2,1)S(1)}, bf16[160,256]{1,0:T(8,128)(2,1)S(1)}, u32[]{:S(2)}, u32[]{:S(2)}) collective-permute-start(bf16[160,256]{1,0:T(8,128)(2,1)S(1)} %shard_map.195.refs_0_), channel_id=1, source_target_pairs={{0,16},{8,24},{16,0},{24,8},{1,17},{9,25},{17,1},{25,9},{2,18},{10... | collective-permute-start | bytes 245768 | tf_op jit(solution)/shard_map/ppermute | solution.py:379
  23.8 6.0 %collective-permute-start.2 = (bf16[160,256]{1,0:T(8,128)(2,1)S(1)}, bf16[160,256]{1,0:T(8,128)(2,1)S(1)}, u32[]{:S(2)}, u32[]{:S(2)}) collective-permute-start(bf16[160,256]{1,0:T(8,128)(2,1)S(1)} %shard_map.195.refs_0_), channel_id=1, source_target_pairs={{0,24},{8,0},{16,8},{24,16},{1,25},{9,1},{17,9},{25,17},{2,26},{10... | collective-permute-start | bytes 245768 | tf_op jit(solution)/shard_map/ppermute | solution.py:379
  27.1 26.4 %collective-permute-start.26 = (bf16[256,1024]{1,0:T(8,128)(2,1)}, bf16[256,1024]{1,0:T(8,128)(2,1)}, u32[]{:S(2)}, u32[]{:S(2)}) collective-permute-start(bf16[256,1024]{1,0:T(8,128)(2,1)} %get-tuple-element.20), channel_id=1, source_target_pairs={{0,3},{1,2},{2,1},{3,0},{4,7},{5,6},{6,5},{7,4},{8,11},{9,10},{10,... | collective-permute-start | bytes 1572872 | tf_op jit(solution)/shard_map/ppermute | solution.py:364
  30.6 20.1 %collective-permute-start.4 = (bf16[4,160,256]{2,1,0:T(8,128)(2,1)}, bf16[4,160,256]{2,1,0:T(8,128)(2,1)}, u32[]{:S(2)}, u32[]{:S(2)}) collective-permute-start(bf16[4,160,256]{2,1,0:T(8,128)(2,1)} %shard_map.196.refs_0_), channel_id=1, source_target_pairs={{0,32},{32,64},{64,96},{96,128},{128,160},{160,192},{192,224},{224... | collective-permute-start | bytes 983048 | tf_op jit(solution)/shard_map/ppermute | solution.py:414
  47.5 18.5 %collective-permute-start.28 = (bf16[256,1024]{1,0:T(8,128)(2,1)S(1)}, bf16[256,1024]{1,0:T(8,128)(2,1)S(1)}, u32[]{:S(2)}, u32[]{:S(2)}) collective-permute-start(bf16[256,1024]{1,0:T(8,128)(2,1)S(1)} %get-tuple-element.22), channel_id=1, source_target_pairs={{0,3},{1,2},{2,1},{3,0},{4,7},{5,6},{6,5},{7,4},{8,11},{9,10},{10,... | collective-permute-start | bytes 1572872 | tf_op jit(solution)/shard_map/ppermute | solution.py:393
  50.7 22.9 %collective-permute-start.21 = (bf16[256,1024]{1,0:T(8,128)(2,1)S(1)}, bf16[256,1024]{1,0:T(8,128)(2,1)S(1)}, u32[]{:S(2)}, u32[]{:S(2)}) collective-permute-start(bf16[256,1024]{1,0:T(8,128)(2,1)S(1)} %get-tuple-element.23), channel_id=1, source_target_pairs={{0,3},{1,2},{2,1},{3,0},{4,7},{5,6},{6,5},{7,4},{8,11},{9,10},{10,... | collective-permute-start | bytes 1572872 | tf_op jit(solution)/shard_map/ppermute | solution.py:393
  53.5 25.1 %collective-permute-start.6 = (bf16[4,160,256]{2,1,0:T(8,128)(2,1)}, bf16[4,160,256]{2,1,0:T(8,128)(2,1)}, u32[]{:S(2)}, u32[]{:S(2)}) collective-permute-start(bf16[4,160,256]{2,1,0:T(8,128)(2,1)} %shard_map.196.refs_0_), channel_id=1, source_target_pairs={{0,224},{32,0},{64,32},{96,64},{128,96},{160,128},{192,160},{224,1... | collective-permute-start | bytes 983048 | tf_op jit(solution)/shard_map/ppermute | solution.py:417
  54.6 24.1 %collective-permute-start.25 = (bf16[256,1024]{1,0:T(8,128)(2,1)S(1)}, bf16[256,1024]{1,0:T(8,128)(2,1)S(1)}, u32[]{:S(2)}, u32[]{:S(2)}) collective-permute-start(bf16[256,1024]{1,0:T(8,128)(2,1)S(1)} %copy-done.3), channel_id=1, source_target_pairs={{0,1},{1,0},{2,3},{3,2},{4,5},{5,4},{6,7},{7,6},{8,9},{9,8},{10,11... | collective-permute-start | bytes 1572872 | tf_op jit(solution)/shard_map/ppermute | solution.py:365
  64.7 22.4 %collective-permute-start.27 = (bf16[256,1024]{1,0:T(8,128)(2,1)}, bf16[256,1024]{1,0:T(8,128)(2,1)S(1)}, u32[]{:S(2)}, u32[]{:S(2)}) collective-permute-start(bf16[256,1024]{1,0:T(8,128)(2,1)} %collective-permute-done.26.w2_ref), channel_id=1, source_target_pairs={{0,1},{1,0},{2,3},{3,2},{4,5},{5,4},{6,7},{7,6},{8,9},{9,8},{10,11... | collective-permute-start | bytes 1572872 | tf_op jit(solution)/shard_map/ppermute | solution.py:366
  66.0 13.6 %collective-permute-start.8 = (bf16[4,160,256]{2,1,0:T(8,128)(2,1)}, bf16[4,160,256]{2,1,0:T(8,128)(2,1)}, u32[]{:S(2)}, u32[]{:S(2)}) collective-permute-start(bf16[4,160,256]{2,1,0:T(8,128)(2,1)} %collective-permute-done.4.refs_2_), channel_id=1, source_target_pairs={{0,32},{32,64},{64,96},{96,128},{128,160},{160,192},{192,224},{224... | collective-permute-start | bytes 983048 | tf_op jit(solution)/shard_map/ppermute | solution.py:414
  73.6 13.5 %collective-permute-start.29 = (bf16[256,512]{1,0:T(8,128)(2,1)S(1)}, bf16[256,512]{1,0:T(8,128)(2,1)S(1)}, u32[]{:S(2)}, u32[]{:S(2)}) collective-permute-start(bf16[256,512]{1,0:T(8,128)(2,1)S(1)} %shard_map.200.a_ref), channel_id=1, source_target_pairs={{0,3},{1,2},{2,1},{3,0},{4,7},{5,6},{6,5},{7,4},{8,11},{9,10},{10,... | collective-permute-start | bytes 786440 | tf_op jit(solution)/shard_map/ppermute | solution.py:400
  78.5 10.3 %collective-permute-start.24 = (bf16[256,512]{1,0:T(8,128)(2,1)S(1)}, bf16[256,512]{1,0:T(8,128)(2,1)S(1)}, u32[]{:S(2)}, u32[]{:S(2)}) collective-permute-start(bf16[256,512]{1,0:T(8,128)(2,1)S(1)} %shard_map.198.a_ref), channel_id=1, source_target_pairs={{0,3},{1,2},{2,1},{3,0},{4,7},{5,6},{6,5},{7,4},{8,11},{9,10},{10,... | collective-permute-start | bytes 786440 | tf_op jit(solution)/shard_map/ppermute | solution.py:400
  78.7 27.7 %collective-permute-start.10 = (bf16[4,160,256]{2,1,0:T(8,128)(2,1)}, bf16[4,160,256]{2,1,0:T(8,128)(2,1)S(1)}, u32[]{:S(2)}, u32[]{:S(2)}) collective-permute-start(bf16[4,160,256]{2,1,0:T(8,128)(2,1)} %collective-permute-done.6.refs_4_), channel_id=1, source_target_pairs={{0,224},{32,0},{64,32},{96,64},{128,96},{160,128},{192,160},{224,1... | collective-permute-start | bytes 983048 | tf_op jit(solution)/shard_map/ppermute | solution.py:417
  79.6 29.5 %collective-permute-start.12 = (bf16[4,160,256]{2,1,0:T(8,128)(2,1)}, bf16[4,160,256]{2,1,0:T(8,128)(2,1)S(1)}, u32[]{:S(2)}, u32[]{:S(2)}) collective-permute-start(bf16[4,160,256]{2,1,0:T(8,128)(2,1)} %collective-permute-done.8.refs_6_), channel_id=1, source_target_pairs={{0,32},{32,64},{64,96},{96,128},{128,160},{160,192},{192,224},{224... | collective-permute-start | bytes 983048 | tf_op jit(solution)/shard_map/ppermute | solution.py:414
  91.7 73.7 %all-to-all-start.1 = ((bf16[128,8,512]{2,1,0:T(8,128)(2,1)}), bf16[128,8,512]{2,1,0:T(8,128)(2,1)S(1)}, u32[]{:S(2)}, u32[]{:S(2)}) async-start(bf16[128,8,512]{2,1,0:T(8,128)(2,1)} %bitcast.12), calls=%async_computation.1 | async-start | bytes 2097152 | tf_op jit(solution)/shard_map/all_to_all | solution.py:445
  104.9 4.2 %collective-permute-start.3 = (bf16[4,160,256]{2,1,0:T(8,128)(2,1)}, bf16[4,160,256]{2,1,0:T(8,128)(2,1)S(1)}, u32[]{:S(2)}, u32[]{:S(2)}) collective-permute-start(bf16[4,160,256]{2,1,0:T(8,128)(2,1)} %shard_map.196.refs_0_), channel_id=1, source_target_pairs={{0,4},{4,0},{1,5},{5,1},{2,6},{6,2},{3,7},{7,3},{8,12},{12,8},{9,1... | collective-permute-start | bytes 983048 | tf_op jit(solution)/shard_map/ppermute | solution.py:421
  105.9 3.7 %collective-permute-start.5 = (bf16[4,160,256]{2,1,0:T(8,128)(2,1)}, bf16[4,160,256]{2,1,0:T(8,128)(2,1)S(1)}, u32[]{:S(2)}, u32[]{:S(2)}) collective-permute-start(bf16[4,160,256]{2,1,0:T(8,128)(2,1)} %collective-permute-done.4.refs_2_), channel_id=1, source_target_pairs={{0,4},{4,0},{1,5},{5,1},{2,6},{6,2},{3,7},{7,3},{8,12},{12,8},{9,1... | collective-permute-start | bytes 983048 | tf_op jit(solution)/shard_map/ppermute | solution.py:421
  106.0 4.0 %collective-permute-start.7 = (bf16[4,160,256]{2,1,0:T(8,128)(2,1)}, bf16[4,160,256]{2,1,0:T(8,128)(2,1)S(1)}, u32[]{:S(2)}, u32[]{:S(2)}) collective-permute-start(bf16[4,160,256]{2,1,0:T(8,128)(2,1)} %collective-permute-done.6.refs_4_), channel_id=1, source_target_pairs={{0,4},{4,0},{1,5},{5,1},{2,6},{6,2},{3,7},{7,3},{8,12},{12,8},{9,1... | collective-permute-start | bytes 983048 | tf_op jit(solution)/shard_map/ppermute | solution.py:421
  106.4 29.4 %collective-permute-start.14 = (bf16[4,160,256]{2,1,0:T(8,128)(2,1)S(1)}, bf16[4,160,256]{2,1,0:T(8,128)(2,1)S(1)}, u32[]{:S(2)}, u32[]{:S(2)}) collective-permute-start(bf16[4,160,256]{2,1,0:T(8,128)(2,1)S(1)} %collective-permute-done.10.refs_8_), channel_id=1, source_target_pairs={{0,224},{32,0},{64,32},{96,64},{128,96},{160,128},{192,160},{224,1... | collective-permute-start | bytes 983048 | tf_op jit(solution)/shard_map/ppermute | solution.py:417
  109.1 28.5 %collective-permute-start.16 = (bf16[4,160,256]{2,1,0:T(8,128)(2,1)S(1)}, bf16[4,160,256]{2,1,0:T(8,128)(2,1)S(1)}, u32[]{:S(2)}, u32[]{:S(2)}) collective-permute-start(bf16[4,160,256]{2,1,0:T(8,128)(2,1)S(1)} %collective-permute-done.12.refs_10_), channel_id=1, source_target_pairs={{0,32},{32,64},{64,96},{96,128},{128,160},{160,192},{192,224},{224... | collective-permute-start | bytes 983048 | tf_op jit(solution)/shard_map/ppermute | solution.py:414
  109.1 29.9 %collective-permute-start.11 = (bf16[4,160,256]{2,1,0:T(8,128)(2,1)S(1)}, bf16[4,160,256]{2,1,0:T(8,128)(2,1)S(1)}, u32[]{:S(2)}, u32[]{:S(2)}) collective-permute-start(bf16[4,160,256]{2,1,0:T(8,128)(2,1)S(1)} %collective-permute-done.10.refs_8_), channel_id=1, source_target_pairs={{0,4},{4,0},{1,5},{5,1},{2,6},{6,2},{3,7},{7,3},{8,12},{12,8},{9,1... | collective-permute-start | bytes 983048 | tf_op jit(solution)/shard_map/ppermute | solution.py:421
  109.6 29.5 %collective-permute-start.9 = (bf16[4,160,256]{2,1,0:T(8,128)(2,1)}, bf16[4,160,256]{2,1,0:T(8,128)(2,1)S(1)}, u32[]{:S(2)}, u32[]{:S(2)}) collective-permute-start(bf16[4,160,256]{2,1,0:T(8,128)(2,1)} %collective-permute-done.8.refs_6_), channel_id=1, source_target_pairs={{0,4},{4,0},{1,5},{5,1},{2,6},{6,2},{3,7},{7,3},{8,12},{12,8},{9,1... | collective-permute-start | bytes 983048 | tf_op jit(solution)/shard_map/ppermute | solution.py:421
  109.9 29.1 %collective-permute-start.13 = (bf16[4,160,256]{2,1,0:T(8,128)(2,1)S(1)}, bf16[4,160,256]{2,1,0:T(8,128)(2,1)S(1)}, u32[]{:S(2)}, u32[]{:S(2)}) collective-permute-start(bf16[4,160,256]{2,1,0:T(8,128)(2,1)S(1)} %collective-permute-done.12.refs_10_), channel_id=1, source_target_pairs={{0,4},{4,0},{1,5},{5,1},{2,6},{6,2},{3,7},{7,3},{8,12},{12,8},{9,1... | collective-permute-start | bytes 983048 | tf_op jit(solution)/shard_map/ppermute | solution.py:421
  135.7 3.3 %collective-permute-start.15 = (bf16[4,160,256]{2,1,0:T(8,128)(2,1)S(1)}, bf16[4,160,256]{2,1,0:T(8,128)(2,1)S(1)}, u32[]{:S(2)}, u32[]{:S(2)}) collective-permute-start(bf16[4,160,256]{2,1,0:T(8,128)(2,1)S(1)} %collective-permute-done.14.refs_12_), channel_id=1, source_target_pairs={{0,4},{4,0},{1,5},{5,1},{2,6},{6,2},{3,7},{7,3},{8,12},{12,8},{9,1... | collective-permute-start | bytes 983048 | tf_op jit(solution)/shard_map/ppermute | solution.py:421
  137.6 2.2 %collective-permute-start.17 = (bf16[4,160,256]{2,1,0:T(8,128)(2,1)S(1)}, bf16[4,160,256]{2,1,0:T(8,128)(2,1)S(1)}, u32[]{:S(2)}, u32[]{:S(2)}) collective-permute-start(bf16[4,160,256]{2,1,0:T(8,128)(2,1)S(1)} %collective-permute-done.16.refs_14_), channel_id=1, source_target_pairs={{0,4},{4,0},{1,5},{5,1},{2,6},{6,2},{3,7},{7,3},{8,12},{12,8},{9,1... | collective-permute-start | bytes 983048 | tf_op jit(solution)/shard_map/ppermute | solution.py:421
  154.8 6.0 %collective-permute-start.18 = (bf16[32,2048]{1,0:T(8,128)(2,1)S(1)}, bf16[32,2048]{1,0:T(8,128)(2,1)S(1)}, u32[]{:S(2)}, u32[]{:S(2)}) collective-permute-start(bf16[32,2048]{1,0:T(8,128)(2,1)S(1)} %get-tuple-element.13), channel_id=1, source_target_pairs={{0,1},{1,2},{2,3},{3,0},{4,5},{5,6},{6,7},{7,4},{8,9},{9,10},{10,1... | collective-permute-start | bytes 393224 | tf_op jit(solution)/shard_map/ppermute | solution.py:442
  156.0 8.7 %collective-permute-start.19 = (bf16[32,2048]{1,0:T(8,128)(2,1)S(1)}, bf16[32,2048]{1,0:T(8,128)(2,1)S(1)}, u32[]{:S(2)}, u32[]{:S(2)}) collective-permute-start(bf16[32,2048]{1,0:T(8,128)(2,1)S(1)} %get-tuple-element.14), channel_id=1, source_target_pairs={{0,2},{1,3},{2,0},{3,1},{4,6},{5,7},{6,4},{7,5},{8,10},{9,11},{10,... | collective-permute-start | bytes 393224 | tf_op jit(solution)/shard_map/ppermute | solution.py:442
  158.7 6.0 %collective-permute-start.20 = (bf16[32,2048]{1,0:T(8,128)(2,1)S(1)}, bf16[32,2048]{1,0:T(8,128)(2,1)S(1)}, u32[]{:S(2)}, u32[]{:S(2)}) collective-permute-start(bf16[32,2048]{1,0:T(8,128)(2,1)S(1)} %get-tuple-element.15), channel_id=1, source_target_pairs={{0,3},{1,0},{2,1},{3,2},{4,7},{5,4},{6,5},{7,6},{8,11},{9,8},{10,9... | collective-permute-start | bytes 393224 | tf_op jit(solution)/shard_map/ppermute | solution.py:442
  (18 other events, 447.8 us)

commit v2 on v1

--- a/solution.py
+++ b/solution.py
@@ -102,7 +102,7 @@
     blocks = kv_ref.shape[1]
     ways = rank // ROPE
     few = tok_rows // ways
-    group = 4
+    group = 8
 
     def step(j, carry):
         latent, turned = [], []
@@ -236,20 +236,23 @@
     other_ref[...] = wd_ref[:, pl.ds(pl.multiple_of((1 - upper) * part, part), part)]
 
 
-def down_kernel(a_ref, b_ref, w0_ref, w1_ref, w2_ref, w3_ref, *rest):
-    out_ref = rest[-1]
+def down_kernel(turn, a_ref, b_ref, w0_ref, w1_ref, w2_ref, w3_ref, *rest):
+    out_hbm, out_ref, sem = rest[-3:]
     units = w0_ref.shape[0]
-    experts, ways, per, part = out_ref.shape
-    fresh = a_ref.shape[0] // per
-    if len(rest) > 1:
-        out_ref[: experts - fresh] = rest[0][...]
+    ways, experts, per, part = out_ref.shape
+    stores = []
     for y in range(ways):
         cols = slice(y * part, (y + 1) * part)
         total = 0.0
         for ref, k, wd_ref in ((a_ref, 0, w0_ref), (a_ref, 1, w1_ref), (b_ref, 0, w2_ref), (b_ref, 1, w3_ref)):
             term = dot(ref[:, k * units : (k + 1) * units], wd_ref[:, cols])
             total = total + term.astype(bf16).astype(f32)
-        out_ref[experts - fresh :, y] = total.astype(bf16).reshape(fresh, per, part)
+        out_ref[y] = total.astype(bf16).reshape(experts, per, part)
+        place = out_hbm.at[pl.ds(turn * experts, experts), y]
+        stores.append(pltpu.make_async_copy(out_ref.at[y], place, sem.at[y]))
+        stores[-1].start()
+    for store in stores:
+        store.wait()
 
 
 def combine_kernel(target_ref, weight_ref, *rest):
@@ -398,13 +401,24 @@
     for i in range(halves):
         hidden = call(hidden_kernel, shape(few, 2 * units), (me, joined[i], *weights, held[i]), 8 * few * part * units)
         far_hidden = lax.ppermute(hidden, TP, across(3))
+        operands = (hidden, far_hidden, *down)
         result = (
-            call(
-                down_kernel,
-                shape(experts * (i + 1) // halves, 2, per, part // 2),
-                (hidden, far_hidden, *down, *result),
-                8 * few * units * part,
-            ),
+            pl.pallas_call(
+                functools.partial(down_kernel, i),
+                out_shape=shape(experts, 2, per, part // 2),
+                in_specs=[vmem()] * len(operands) + [far] * len(result),
+                out_specs=far,
+                scratch_shapes=[
+                    pltpu.VMEM((2, experts // halves, per, part // 2), bf16),
+                    pltpu.SemaphoreType.DMA((2,)),
+                ],
+                input_output_aliases={len(operands): 0} if result else {},
+                compiler_params=params(48),
+                cost_estimate=pl.CostEstimate(
+                    flops=8 * few * units * part, transcendentals=0, bytes_accessed=4 * 10**6
+                ),
+                name="down",
+            )(*operands, *result),
         )
     result = result[0]
 
@@ -439,7 +453,9 @@
         cost_estimate=pl.CostEstimate(flops=6 * 10**9, transcendentals=0, bytes_accessed=8 * 10**6),
         name="attend",
     )(me, queries, w_key, w_value, w_out, *pieces)
-    held = [shares[0]] + [lax.ppermute(s, TP, ahead(k)) for k, s in enumerate(shares) if k]
+    held = [shares[0]]
+    for k in range(1, tp):
+        held.append(lax.ppermute(shares[k], TP, ahead(k)))
     mixer_out = sum(s.astype(f32) for s in held).astype(bf16)
 
     returned = lax.all_to_all(result.reshape(2 * experts, per, part // 2), (*EP, "yl"), 0, 0, tiled=True)

time: 168 us -> 168 us (level)
    pallas_call x0 -> x2, Pallas kernels: none -> 5.02 us  [inner(): pl.pallas_call(functools.partial(down_kernel, i), out_shape=shape(experts...]
    pallas_call x10 -> x8, Pallas kernels: 16.3 us -> 11.7 us  [call(): pl.pallas_call(kernel, out_shape=out_shape, in_specs=[smem() if a.size ==...]
where the time goes in v2:
time: 168 us; the launch traced here: 167 us
  waiting for transfers between devices  65.2 us (39%)
  starting transfers between devices  63.2 us (38%)
  Pallas kernels  34.1 us (20%)
  local copies, waits for them, and re-layouts  2.75 us (2%)
    ppermute x3, waiting for transfers between devices, inner(): low = lax.ppermute(low, 'z', ahead(depth - 1, depth))  25.6 us
    all_to_all x1, waiting for transfers between devices, inner(): arrived = lax.all_to_all(outgoing, EP, 0, 0, tiled=True)  14.6 us
    pallas_call x1, Pallas kernels, inner(): pl.pallas_call(functools.partial(attend_kernel, count), out_shape=[share]...  14.2 us
    all_to_all x1, starting transfers between devices, inner(): lax.all_to_all(result.reshape(2 * experts, per, part // 2), (*EP, 'yl'),...  13.2 us
    all_to_all x1, starting transfers between devices, inner(): arrived = lax.all_to_all(outgoing, EP, 0, 0, tiled=True)  13 us
    pallas_call x8, Pallas kernels, call(): pl.pallas_call(kernel, out_shape=out_shape, in_specs=[smem() if a.size ==...  11.7 us
    ppermute x1, waiting for transfers between devices, inner(): far_up = lax.ppermute(w_up[0], TP, across(1))  10.1 us
    ppermute x1, waiting for transfers between devices, inner(): down2 = lax.ppermute(down3, TP, across(1))  6.88 us
  transfers between devices with their start and end apart: 32, of which 10 were waited for; matrix products, arithmetic and copies ran while one was open for 1% of the time, Pallas kernels for 17%

profile of v2, /device:TPU:1, one launch (start us, length us, event | category | flops | bytes accessed | tf_op | source)
XLA Modules:
  0.0 167.3 jit_solution(1486574143014129680)
XLA Ops:
  0.7 3.1 %prep.1 = (s32[2,512]{1,0:T(2,128)S(1)}, bf16[64,8,1024]{2,1,0:T(8,128)(2,1)S(1)}) custom-call(s32[1]{0:T(128)} %bitcast.me_ref, bf16[512,2048]{1,0:T(8,128)(2,1)} %tok_hbm.1, f32[1,2048]{1,0:T(1,128)} %bitcast.30, s32[2,512]{1,0:T(2,128)} %bitcast.31), custom_call_target="tpu_custom_call" | custom-call | flops 600000000 | bytes 4000000 | tf_op jit(solution)/shard_map/prep/pallas_call | solution.py:340
  4.8 13.0 %all-to-all-start = ((bf16[64,8,1024]{2,1,0:T(8,128)(2,1)}), bf16[64,8,1024]{2,1,0:T(8,128)(2,1)S(1)}, u32[]{:S(2)}, u32[]{:S(2)}) async-start(bf16[64,8,1024]{2,1,0:T(8,128)(2,1)} %copy-done.5), calls=%async_computation | async-start | bytes 2097152 | tf_op jit(solution)/shard_map/all_to_all | solution.py:363
  17.8 1.4 collective-permute-start.22
  20.1 1.4 collective-permute-start
  21.4 2.4 %collective-permute-start.1 = (bf16[160,256]{1,0:T(8,128)(2,1)S(1)}, bf16[160,256]{1,0:T(8,128)(2,1)S(1)}, u32[]{:S(2)}, u32[]{:S(2)}) collective-permute-start(bf16[160,256]{1,0:T(8,128)(2,1)S(1)} %shard_map.195.refs_0_), channel_id=1, source_target_pairs={{0,16},{8,24},{16,0},{24,8},{1,17},{9,25},{17,1},{25,9},{2,18},{10... | collective-permute-start | bytes 245768 | tf_op jit(solution)/shard_map/ppermute | solution.py:382
  23.8 1.2 collective-permute-start.2
  25.0 1.2 copy-done.4
  27.1 2.7 %collective-permute-start.26 = (bf16[256,1024]{1,0:T(8,128)(2,1)}, bf16[256,1024]{1,0:T(8,128)(2,1)}, u32[]{:S(2)}, u32[]{:S(2)}) collective-permute-start(bf16[256,1024]{1,0:T(8,128)(2,1)} %get-tuple-element.20), channel_id=1, source_target_pairs={{0,3},{1,2},{2,1},{3,0},{4,7},{5,6},{6,5},{7,4},{8,11},{9,10},{10,... | collective-permute-start | bytes 1572872 | tf_op jit(solution)/shard_map/ppermute | solution.py:367
  30.6 2.2 %collective-permute-start.4 = (bf16[4,160,256]{2,1,0:T(8,128)(2,1)}, bf16[4,160,256]{2,1,0:T(8,128)(2,1)}, u32[]{:S(2)}, u32[]{:S(2)}) collective-permute-start(bf16[4,160,256]{2,1,0:T(8,128)(2,1)} %shard_map.196.refs_0_), channel_id=1, source_target_pairs={{0,32},{32,64},{64,96},{96,128},{128,160},{160,192},{192,224},{224... | collective-permute-start | bytes 983048 | tf_op jit(solution)/shard_map/ppermute | solution.py:428
  32.9 14.6 %all-to-all-done = bf16[64,8,1024]{2,1,0:T(8,128)(2,1)S(1)} async-done(((bf16[64,8,1024]{2,1,0:T(8,128)(2,1)}), bf16[64,8,1024]{2,1,0:T(8,128)(2,1)S(1)}, u32[]{:S(2)}, u32[]{:S(2)}) %all-to-all-start) | async-done | bytes 1048608 | tf_op jit(solution)/shard_map/all_to_all | solution.py:363
  47.5 2.8 %collective-permute-start.28 = (bf16[256,1024]{1,0:T(8,128)(2,1)S(1)}, bf16[256,1024]{1,0:T(8,128)(2,1)S(1)}, u32[]{:S(2)}, u32[]{:S(2)}) collective-permute-start(bf16[256,1024]{1,0:T(8,128)(2,1)S(1)} %get-tuple-element.22), channel_id=1, source_target_pairs={{0,3},{1,2},{2,1},{3,0},{4,7},{5,6},{6,5},{7,4},{8,11},{9,10},{10,... | collective-permute-start | bytes 1572872 | tf_op jit(solution)/shard_map/ppermute | solution.py:396
  50.7 2.7 %collective-permute-start.21 = (bf16[256,1024]{1,0:T(8,128)(2,1)S(1)}, bf16[256,1024]{1,0:T(8,128)(2,1)S(1)}, u32[]{:S(2)}, u32[]{:S(2)}) collective-permute-start(bf16[256,1024]{1,0:T(8,128)(2,1)S(1)} %get-tuple-element.23), channel_id=1, source_target_pairs={{0,3},{1,2},{2,1},{3,0},{4,7},{5,6},{6,5},{7,4},{8,11},{9,10},{10,... | collective-permute-start | bytes 1572872 | tf_op jit(solution)/shard_map/ppermute | solution.py:396
  53.5 1.1 collective-permute-start.6
  54.6 10.1 %collective-permute-done.23.vu_ref = bf16[2048,256]{1,0:T(8,128)(2,1)} collective-permute-done((bf16[2048,256]{1,0:T(8,128)(2,1)S(1)}, bf16[2048,256]{1,0:T(8,128)(2,1)}, u32[]{:S(2)}, u32[]{:S(2)}) %collective-permute-start.23) | collective-permute-done | bytes 1048608 | tf_op jit(solution)/shard_map/ppermute | solution.py:332
  64.7 1.3 collective-permute-start.27
  66.0 1.4 collective-permute-start.8
  67.4 2.8 %shard_map.197 = (f32[256,1024]{1,0:T(8,128)S(1)}, f32[256,1024]{1,0:T(8,128)S(1)}) custom-call(s32[1]{0:T(128)} %bitcast.me_ref, bf16[512,1024]{1,0:T(8,128)(2,1)S(1)} %bitcast.16, bf16[2048,256]{1,0:T(8,128)(2,1)S(1)} %bitcast.18, bf16[2048,256]{1,0:T(8,128)(2,1)S(1)} %bitcast.22, bf16[2048,256]{1,0:T(8,128)(2,1)} %collective-permute-done.22.vg_ref, ...), custom_call_target="tpu_custom_call" | custom-call | flops 1073741824 | bytes 7340036 | tf_op jit(solution)/shard_map/pallas_call | solution.py:287
  70.2 2.3 %shard_map.200.a_ref = bf16[256,512]{1,0:T(8,128)(2,1)S(1)} custom-call(s32[1]{0:T(128)} %bitcast.me_ref, bf16[256,1024]{1,0:T(8,128)(2,1)S(1)} %collective-permute-done.28.b_ref, bf16[2048,256]{1,0:T(8,128)(2,1)S(1)} %bitcast.19, bf16[2048,256]{1,0:T(8,128)(2,1)S(1)} %bitcast.23, bf16[2048,256]{1,0:T(8,128)(2,1)} %collective-permute-done.22.vg_ref, ...), custom_call_target="tpu_custom_call" | custom-call | flops 536870912 | bytes 6029316 | tf_op jit(solution)/shard_map/pallas_call | solution.py:287
  72.5 1.1 collective-permute-done.21.b_ref
  73.6 2.6 %collective-permute-start.29 = (bf16[256,512]{1,0:T(8,128)(2,1)S(1)}, bf16[256,512]{1,0:T(8,128)(2,1)S(1)}, u32[]{:S(2)}, u32[]{:S(2)}) collective-permute-start(bf16[256,512]{1,0:T(8,128)(2,1)S(1)} %shard_map.200.a_ref), channel_id=1, source_target_pairs={{0,3},{1,2},{2,1},{3,0},{4,7},{5,6},{6,5},{7,4},{8,11},{9,10},{10,... | collective-permute-start | bytes 786440 | tf_op jit(solution)/shard_map/ppermute | solution.py:403
  76.2 2.3 %shard_map.198.a_ref = bf16[256,512]{1,0:T(8,128)(2,1)S(1)} custom-call(s32[1]{0:T(128)} %bitcast.me_ref, bf16[256,1024]{1,0:T(8,128)(2,1)S(1)} %collective-permute-done.21.b_ref, bf16[2048,256]{1,0:T(8,128)(2,1)S(1)} %bitcast.20, bf16[2048,256]{1,0:T(8,128)(2,1)S(1)} %bitcast.24, bf16[2048,256]{1,0:T(8,128)(2,1)} %collective-permute-done.22.vg_ref, ...), custom_call_target="tpu_custom_call" | custom-call | flops 536870912 | bytes 6029316 | tf_op jit(solution)/shard_map/pallas_call | solution.py:287
  80.2 6.9 %collective-permute-done.27.w3_ref = bf16[256,1024]{1,0:T(8,128)(2,1)S(1)} collective-permute-done((bf16[256,1024]{1,0:T(8,128)(2,1)}, bf16[256,1024]{1,0:T(8,128)(2,1)S(1)}, u32[]{:S(2)}, u32[]{:S(2)}) %collective-permute-start.27) | collective-permute-done | bytes 524320 | tf_op jit(solution)/shard_map/ppermute | solution.py:369
  87.1 2.5 %down.2.rest_0_ = bf16[64,2,8,512]{3,2,1,0:T(8,128)(2,1)} custom-call(bf16[256,512]{1,0:T(8,128)(2,1)S(1)} %shard_map.200.a_ref, bf16[256,512]{1,0:T(8,128)(2,1)S(1)} %collective-permute-done.29.b_ref, bf16[256,1024]{1,0:T(8,128)(2,1)S(1)} %copy-done.3, bf16[256,1024]{1,0:T(8,128)(2,1)S(1)} %collective-permute-done.25.w1_ref, ...), custom_call_target="tpu_custom_call" | custom-call | flops 536870912 | bytes 4000000 | tf_op jit(solution)/shard_map/down/pallas_call | solution.py:406
  89.6 2.5 %down.3 = bf16[64,2,8,512]{3,2,1,0:T(8,128)(2,1)} custom-call(bf16[256,512]{1,0:T(8,128)(2,1)S(1)} %shard_map.198.a_ref, bf16[256,512]{1,0:T(8,128)(2,1)S(1)} %collective-permute-done.24.b_ref, bf16[256,1024]{1,0:T(8,128)(2,1)S(1)} %copy-done.3, bf16[256,1024]{1,0:T(8,128)(2,1)S(1)} %collective-permute-done.25.w1_ref, ...), custom_call_target="tpu_custom_call", output_to_operand_aliasing={{}: (6, {})} | custom-call | flops 536870912 | bytes 4000000 | tf_op jit(solution)/shard_map/down/pallas_call | solution.py:406
  92.2 13.2 %all-to-all-start.1 = ((bf16[128,8,512]{2,1,0:T(8,128)(2,1)}), bf16[128,8,512]{2,1,0:T(8,128)(2,1)S(1)}, u32[]{:S(2)}, u32[]{:S(2)}) async-start(bf16[128,8,512]{2,1,0:T(8,128)(2,1)} %bitcast.12), calls=%async_computation.1 | async-start | bytes 2097152 | tf_op jit(solution)/shard_map/all_to_all | solution.py:461
  106.9 2.7 %collective-permute-start.14 = (bf16[4,160,256]{2,1,0:T(8,128)(2,1)S(1)}, bf16[4,160,256]{2,1,0:T(8,128)(2,1)S(1)}, u32[]{:S(2)}, u32[]{:S(2)}) collective-permute-start(bf16[4,160,256]{2,1,0:T(8,128)(2,1)S(1)} %collective-permute-done.10.refs_8_), channel_id=1, source_target_pairs={{0,224},{32,0},{64,32},{96,64},{128,96},{160,128},{192,160},{224,1... | collective-permute-start | bytes 983048 | tf_op jit(solution)/shard_map/ppermute | solution.py:431
  110.6 25.6 %collective-permute-done.14.refs_12_ = bf16[4,160,256]{2,1,0:T(8,128)(2,1)S(1)} collective-permute-done((bf16[4,160,256]{2,1,0:T(8,128)(2,1)S(1)}, bf16[4,160,256]{2,1,0:T(8,128)(2,1)S(1)}, u32[]{:S(2)}, u32[]{:S(2)}) %collective-permute-start.14) | collective-permute-done | bytes 327712 | tf_op jit(solution)/shard_map/ppermute | solution.py:431
  140.3 14.2 %attend.1 = (bf16[32,2048]{1,0:T(8,128)(2,1)S(1)}, bf16[32,2048]{1,0:T(8,128)(2,1)S(1)}, bf16[32,2048]{1,0:T(8,128)(2,1)S(1)}, bf16[32,2048]{1,0:T(8,128)(2,1)S(1)}) custom-call(s32[1]{0:T(128)} %bitcast.me_ref, bf16[2,128,256]{2,1,0:T(8,128)(2,1)S(1)} %shard_map.194.q_ref, bf16[256,256]{1,0:T(8,128)(2,1)S(1)} %copy-done.12, ...), custom_call_target="tpu_custom_call" | custom-call | flops 6000000000 | bytes 8000000 | tf_op jit(solution)/shard_map/attend/pallas_call | solution.py:439
  154.6 1.3 collective-permute-start.18
  155.8 2.6 %collective-permute-start.19 = (bf16[32,2048]{1,0:T(8,128)(2,1)S(1)}, bf16[32,2048]{1,0:T(8,128)(2,1)S(1)}, u32[]{:S(2)}, u32[]{:S(2)}) collective-permute-start(bf16[32,2048]{1,0:T(8,128)(2,1)S(1)} %get-tuple-element.14), channel_id=1, source_target_pairs={{0,2},{1,3},{2,0},{3,1},{4,6},{5,7},{6,4},{7,5},{8,10},{9,11},{10,... | collective-permute-start | bytes 393224 | tf_op jit(solution)/shard_map/ppermute | solution.py:458
  160.5 4.0 %collective-permute-done.19 = bf16[32,2048]{1,0:T(8,128)(2,1)S(1)} collective-permute-done((bf16[32,2048]{1,0:T(8,128)(2,1)S(1)}, bf16[32,2048]{1,0:T(8,128)(2,1)S(1)}, u32[]{:S(2)}, u32[]{:S(2)}) %collective-permute-start.19) | collective-permute-done | bytes 131104 | tf_op jit(solution)/shard_map/ppermute | solution.py:458
  165.2 2.1 %shard_map.201 = bf16[512,512]{1,0:T(8,128)(2,1)} custom-call(s32[512,2]{1,0:T(8,128)S(1)} %bitcast.27, f32[512,2]{1,0:T(8,128)S(1)} %copy.24.weight_ref, bf16[1024,512]{1,0:T(8,128)(2,1)S(1)} %bitcast.26), custom_call_target="tpu_custom_call" | custom-call | flops 1073741824 | bytes 1581056 | tf_op jit(solution)/shard_map/pallas_call | solution.py:287
  (87 shorter events, 15.0 us)
Async XLA Ops:
  4.8 42.6 %all-to-all-start = ((bf16[64,8,1024]{2,1,0:T(8,128)(2,1)}), bf16[64,8,1024]{2,1,0:T(8,128)(2,1)S(1)}, u32[]{:S(2)}, u32[]{:S(2)}) async-start(bf16[64,8,1024]{2,1,0:T(8,128)(2,1)} %copy-done.5), calls=%async_computation | async-start | bytes 2097152 | tf_op jit(solution)/shard_map/all_to_all | solution.py:363
  17.8 36.8 %collective-permute-start.22 = (bf16[2048,256]{1,0:T(8,128)(2,1)S(1)}, bf16[2048,256]{1,0:T(8,128)(2,1)}, u32[]{:S(2)}, u32[]{:S(2)}) collective-permute-start(bf16[2048,256]{1,0:T(8,128)(2,1)S(1)} %bitcast.17), channel_id=1, source_target_pairs={{0,1},{1,0},{2,3},{3,2},{4,5},{5,4},{6,7},{7,6},{8,9},{9,8},{10,11... | collective-permute-start | bytes 3145736 | tf_op jit(solution)/shard_map/ppermute | solution.py:331
  19.2 45.5 %collective-permute-start.23 = (bf16[2048,256]{1,0:T(8,128)(2,1)S(1)}, bf16[2048,256]{1,0:T(8,128)(2,1)}, u32[]{:S(2)}, u32[]{:S(2)}) collective-permute-start(bf16[2048,256]{1,0:T(8,128)(2,1)S(1)} %bitcast.21), channel_id=1, source_target_pairs={{0,1},{1,0},{2,3},{3,2},{4,5},{5,4},{6,7},{7,6},{8,9},{9,8},{10,11... | collective-permute-start | bytes 3145736 | tf_op jit(solution)/shard_map/ppermute | solution.py:332
  20.1 7.0 %collective-permute-start = (bf16[160,256]{1,0:T(8,128)(2,1)S(1)}, bf16[160,256]{1,0:T(8,128)(2,1)S(1)}, u32[]{:S(2)}, u32[]{:S(2)}) collective-permute-start(bf16[160,256]{1,0:T(8,128)(2,1)S(1)} %shard_map.195.refs_0_), channel_id=1, source_target_pairs={{0,8},{8,16},{16,24},{24,0},{1,9},{9,17},{17,25},{25,1},{2,10},{10... | collective-permute-start | bytes 245768 | tf_op jit(solution)/shard_map/ppermute | solution.py:382
  21.4 8.4 %collective-permute-start.1 = (bf16[160,256]{1,0:T(8,128)(2,1)S(1)}, bf16[160,256]{1,0:T(8,128)(2,1)S(1)}, u32[]{:S(2)}, u32[]{:S(2)}) collective-permute-start(bf16[160,256]{1,0:T(8,128)(2,1)S(1)} %shard_map.195.refs_0_), channel_id=1, source_target_pairs={{0,16},{8,24},{16,0},{24,8},{1,17},{9,25},{17,1},{25,9},{2,18},{10... | collective-permute-start | bytes 245768 | tf_op jit(solution)/shard_map/ppermute | solution.py:382
  23.8 6.0 %collective-permute-start.2 = (bf16[160,256]{1,0:T(8,128)(2,1)S(1)}, bf16[160,256]{1,0:T(8,128)(2,1)S(1)}, u32[]{:S(2)}, u32[]{:S(2)}) collective-permute-start(bf16[160,256]{1,0:T(8,128)(2,1)S(1)} %shard_map.195.refs_0_), channel_id=1, source_target_pairs={{0,24},{8,0},{16,8},{24,16},{1,25},{9,1},{17,9},{25,17},{2,26},{10... | collective-permute-start | bytes 245768 | tf_op jit(solution)/shard_map/ppermute | solution.py:382
  27.1 26.4 %collective-permute-start.26 = (bf16[256,1024]{1,0:T(8,128)(2,1)}, bf16[256,1024]{1,0:T(8,128)(2,1)}, u32[]{:S(2)}, u32[]{:S(2)}) collective-permute-start(bf16[256,1024]{1,0:T(8,128)(2,1)} %get-tuple-element.20), channel_id=1, source_target_pairs={{0,3},{1,2},{2,1},{3,0},{4,7},{5,6},{6,5},{7,4},{8,11},{9,10},{10,... | collective-permute-start | bytes 1572872 | tf_op jit(solution)/shard_map/ppermute | solution.py:367
  30.6 20.1 %collective-permute-start.4 = (bf16[4,160,256]{2,1,0:T(8,128)(2,1)}, bf16[4,160,256]{2,1,0:T(8,128)(2,1)}, u32[]{:S(2)}, u32[]{:S(2)}) collective-permute-start(bf16[4,160,256]{2,1,0:T(8,128)(2,1)} %shard_map.196.refs_0_), channel_id=1, source_target_pairs={{0,32},{32,64},{64,96},{96,128},{128,160},{160,192},{192,224},{224... | collective-permute-start | bytes 983048 | tf_op jit(solution)/shard_map/ppermute | solution.py:428
  47.5 18.5 %collective-permute-start.28 = (bf16[256,1024]{1,0:T(8,128)(2,1)S(1)}, bf16[256,1024]{1,0:T(8,128)(2,1)S(1)}, u32[]{:S(2)}, u32[]{:S(2)}) collective-permute-start(bf16[256,1024]{1,0:T(8,128)(2,1)S(1)} %get-tuple-element.22), channel_id=1, source_target_pairs={{0,3},{1,2},{2,1},{3,0},{4,7},{5,6},{6,5},{7,4},{8,11},{9,10},{10,... | collective-permute-start | bytes 1572872 | tf_op jit(solution)/shard_map/ppermute | solution.py:396
  50.7 22.9 %collective-permute-start.21 = (bf16[256,1024]{1,0:T(8,128)(2,1)S(1)}, bf16[256,1024]{1,0:T(8,128)(2,1)S(1)}, u32[]{:S(2)}, u32[]{:S(2)}) collective-permute-start(bf16[256,1024]{1,0:T(8,128)(2,1)S(1)} %get-tuple-element.23), channel_id=1, source_target_pairs={{0,3},{1,2},{2,1},{3,0},{4,7},{5,6},{6,5},{7,4},{8,11},{9,10},{10,... | collective-permute-start | bytes 1572872 | tf_op jit(solution)/shard_map/ppermute | solution.py:396
  53.5 25.1 %collective-permute-start.6 = (bf16[4,160,256]{2,1,0:T(8,128)(2,1)}, bf16[4,160,256]{2,1,0:T(8,128)(2,1)}, u32[]{:S(2)}, u32[]{:S(2)}) collective-permute-start(bf16[4,160,256]{2,1,0:T(8,128)(2,1)} %shard_map.196.refs_0_), channel_id=1, source_target_pairs={{0,224},{32,0},{64,32},{96,64},{128,96},{160,128},{192,160},{224,1... | collective-permute-start | bytes 983048 | tf_op jit(solution)/shard_map/ppermute | solution.py:431
  54.6 24.1 %collective-permute-start.25 = (bf16[256,1024]{1,0:T(8,128)(2,1)S(1)}, bf16[256,1024]{1,0:T(8,128)(2,1)S(1)}, u32[]{:S(2)}, u32[]{:S(2)}) collective-permute-start(bf16[256,1024]{1,0:T(8,128)(2,1)S(1)} %copy-done.3), channel_id=1, source_target_pairs={{0,1},{1,0},{2,3},{3,2},{4,5},{5,4},{6,7},{7,6},{8,9},{9,8},{10,11... | collective-permute-start | bytes 1572872 | tf_op jit(solution)/shard_map/ppermute | solution.py:368
  64.7 22.4 %collective-permute-start.27 = (bf16[256,1024]{1,0:T(8,128)(2,1)}, bf16[256,1024]{1,0:T(8,128)(2,1)S(1)}, u32[]{:S(2)}, u32[]{:S(2)}) collective-permute-start(bf16[256,1024]{1,0:T(8,128)(2,1)} %collective-permute-done.26.w2_ref), channel_id=1, source_target_pairs={{0,1},{1,0},{2,3},{3,2},{4,5},{5,4},{6,7},{7,6},{8,9},{9,8},{10,11... | collective-permute-start | bytes 1572872 | tf_op jit(solution)/shard_map/ppermute | solution.py:369
  66.0 13.6 %collective-permute-start.8 = (bf16[4,160,256]{2,1,0:T(8,128)(2,1)}, bf16[4,160,256]{2,1,0:T(8,128)(2,1)}, u32[]{:S(2)}, u32[]{:S(2)}) collective-permute-start(bf16[4,160,256]{2,1,0:T(8,128)(2,1)} %collective-permute-done.4.refs_2_), channel_id=1, source_target_pairs={{0,32},{32,64},{64,96},{96,128},{128,160},{160,192},{192,224},{224... | collective-permute-start | bytes 983048 | tf_op jit(solution)/shard_map/ppermute | solution.py:428
  73.6 13.5 %collective-permute-start.29 = (bf16[256,512]{1,0:T(8,128)(2,1)S(1)}, bf16[256,512]{1,0:T(8,128)(2,1)S(1)}, u32[]{:S(2)}, u32[]{:S(2)}) collective-permute-start(bf16[256,512]{1,0:T(8,128)(2,1)S(1)} %shard_map.200.a_ref), channel_id=1, source_target_pairs={{0,3},{1,2},{2,1},{3,0},{4,7},{5,6},{6,5},{7,4},{8,11},{9,10},{10,... | collective-permute-start | bytes 786440 | tf_op jit(solution)/shard_map/ppermute | solution.py:403
  78.5 11.1 %collective-permute-start.24 = (bf16[256,512]{1,0:T(8,128)(2,1)S(1)}, bf16[256,512]{1,0:T(8,128)(2,1)S(1)}, u32[]{:S(2)}, u32[]{:S(2)}) collective-permute-start(bf16[256,512]{1,0:T(8,128)(2,1)S(1)} %shard_map.198.a_ref), channel_id=1, source_target_pairs={{0,3},{1,2},{2,1},{3,0},{4,7},{5,6},{6,5},{7,4},{8,11},{9,10},{10,... | collective-permute-start | bytes 786440 | tf_op jit(solution)/shard_map/ppermute | solution.py:403
  78.7 28.2 %collective-permute-start.10 = (bf16[4,160,256]{2,1,0:T(8,128)(2,1)}, bf16[4,160,256]{2,1,0:T(8,128)(2,1)S(1)}, u32[]{:S(2)}, u32[]{:S(2)}) collective-permute-start(bf16[4,160,256]{2,1,0:T(8,128)(2,1)} %collective-permute-done.6.refs_4_), channel_id=1, source_target_pairs={{0,224},{32,0},{64,32},{96,64},{128,96},{160,128},{192,160},{224,1... | collective-permute-start | bytes 983048 | tf_op jit(solution)/shard_map/ppermute | solution.py:431
  79.6 30.0 %collective-permute-start.12 = (bf16[4,160,256]{2,1,0:T(8,128)(2,1)}, bf16[4,160,256]{2,1,0:T(8,128)(2,1)S(1)}, u32[]{:S(2)}, u32[]{:S(2)}) collective-permute-start(bf16[4,160,256]{2,1,0:T(8,128)(2,1)} %collective-permute-done.8.refs_6_), channel_id=1, source_target_pairs={{0,32},{32,64},{64,96},{96,128},{128,160},{160,192},{192,224},{224... | collective-permute-start | bytes 983048 | tf_op jit(solution)/shard_map/ppermute | solution.py:428
  92.2 73.0 %all-to-all-start.1 = ((bf16[128,8,512]{2,1,0:T(8,128)(2,1)}), bf16[128,8,512]{2,1,0:T(8,128)(2,1)S(1)}, u32[]{:S(2)}, u32[]{:S(2)}) async-start(bf16[128,8,512]{2,1,0:T(8,128)(2,1)} %bitcast.12), calls=%async_computation.1 | async-start | bytes 2097152 | tf_op jit(solution)/shard_map/all_to_all | solution.py:461
  105.4 4.2 %collective-permute-start.3 = (bf16[4,160,256]{2,1,0:T(8,128)(2,1)}, bf16[4,160,256]{2,1,0:T(8,128)(2,1)S(1)}, u32[]{:S(2)}, u32[]{:S(2)}) collective-permute-start(bf16[4,160,256]{2,1,0:T(8,128)(2,1)} %shard_map.196.refs_0_), channel_id=1, source_target_pairs={{0,4},{4,0},{1,5},{5,1},{2,6},{6,2},{3,7},{7,3},{8,12},{12,8},{9,1... | collective-permute-start | bytes 983048 | tf_op jit(solution)/shard_map/ppermute | solution.py:435
  106.4 3.7 %collective-permute-start.5 = (bf16[4,160,256]{2,1,0:T(8,128)(2,1)}, bf16[4,160,256]{2,1,0:T(8,128)(2,1)S(1)}, u32[]{:S(2)}, u32[]{:S(2)}) collective-permute-start(bf16[4,160,256]{2,1,0:T(8,128)(2,1)} %collective-permute-done.4.refs_2_), channel_id=1, source_target_pairs={{0,4},{4,0},{1,5},{5,1},{2,6},{6,2},{3,7},{7,3},{8,12},{12,8},{9,1... | collective-permute-start | bytes 983048 | tf_op jit(solution)/shard_map/ppermute | solution.py:435
  106.5 4.0 %collective-permute-start.7 = (bf16[4,160,256]{2,1,0:T(8,128)(2,1)}, bf16[4,160,256]{2,1,0:T(8,128)(2,1)S(1)}, u32[]{:S(2)}, u32[]{:S(2)}) collective-permute-start(bf16[4,160,256]{2,1,0:T(8,128)(2,1)} %collective-permute-done.6.refs_4_), channel_id=1, source_target_pairs={{0,4},{4,0},{1,5},{5,1},{2,6},{6,2},{3,7},{7,3},{8,12},{12,8},{9,1... | collective-permute-start | bytes 983048 | tf_op jit(solution)/shard_map/ppermute | solution.py:435
  106.9 29.4 %collective-permute-start.14 = (bf16[4,160,256]{2,1,0:T(8,128)(2,1)S(1)}, bf16[4,160,256]{2,1,0:T(8,128)(2,1)S(1)}, u32[]{:S(2)}, u32[]{:S(2)}) collective-permute-start(bf16[4,160,256]{2,1,0:T(8,128)(2,1)S(1)} %collective-permute-done.10.refs_8_), channel_id=1, source_target_pairs={{0,224},{32,0},{64,32},{96,64},{128,96},{160,128},{192,160},{224,1... | collective-permute-start | bytes 983048 | tf_op jit(solution)/shard_map/ppermute | solution.py:431
  109.6 28.5 %collective-permute-start.16 = (bf16[4,160,256]{2,1,0:T(8,128)(2,1)S(1)}, bf16[4,160,256]{2,1,0:T(8,128)(2,1)S(1)}, u32[]{:S(2)}, u32[]{:S(2)}) collective-permute-start(bf16[4,160,256]{2,1,0:T(8,128)(2,1)S(1)} %collective-permute-done.12.refs_10_), channel_id=1, source_target_pairs={{0,32},{32,64},{64,96},{96,128},{128,160},{160,192},{192,224},{224... | collective-permute-start | bytes 983048 | tf_op jit(solution)/shard_map/ppermute | solution.py:428
  109.6 29.9 %collective-permute-start.11 = (bf16[4,160,256]{2,1,0:T(8,128)(2,1)S(1)}, bf16[4,160,256]{2,1,0:T(8,128)(2,1)S(1)}, u32[]{:S(2)}, u32[]{:S(2)}) collective-permute-start(bf16[4,160,256]{2,1,0:T(8,128)(2,1)S(1)} %collective-permute-done.10.refs_8_), channel_id=1, source_target_pairs={{0,4},{4,0},{1,5},{5,1},{2,6},{6,2},{3,7},{7,3},{8,12},{12,8},{9,1... | collective-permute-start | bytes 983048 | tf_op jit(solution)/shard_map/ppermute | solution.py:435
  110.1 29.5 %collective-permute-start.9 = (bf16[4,160,256]{2,1,0:T(8,128)(2,1)}, bf16[4,160,256]{2,1,0:T(8,128)(2,1)S(1)}, u32[]{:S(2)}, u32[]{:S(2)}) collective-permute-start(bf16[4,160,256]{2,1,0:T(8,128)(2,1)} %collective-permute-done.8.refs_6_), channel_id=1, source_target_pairs={{0,4},{4,0},{1,5},{5,1},{2,6},{6,2},{3,7},{7,3},{8,12},{12,8},{9,1... | collective-permute-start | bytes 983048 | tf_op jit(solution)/shard_map/ppermute | solution.py:435
  110.4 29.1 %collective-permute-start.13 = (bf16[4,160,256]{2,1,0:T(8,128)(2,1)S(1)}, bf16[4,160,256]{2,1,0:T(8,128)(2,1)S(1)}, u32[]{:S(2)}, u32[]{:S(2)}) collective-permute-start(bf16[4,160,256]{2,1,0:T(8,128)(2,1)S(1)} %collective-permute-done.12.refs_10_), channel_id=1, source_target_pairs={{0,4},{4,0},{1,5},{5,1},{2,6},{6,2},{3,7},{7,3},{8,12},{12,8},{9,1... | collective-permute-start | bytes 983048 | tf_op jit(solution)/shard_map/ppermute | solution.py:435
  136.2 3.3 %collective-permute-start.15 = (bf16[4,160,256]{2,1,0:T(8,128)(2,1)S(1)}, bf16[4,160,256]{2,1,0:T(8,128)(2,1)S(1)}, u32[]{:S(2)}, u32[]{:S(2)}) collective-permute-start(bf16[4,160,256]{2,1,0:T(8,128)(2,1)S(1)} %collective-permute-done.14.refs_12_), channel_id=1, source_target_pairs={{0,4},{4,0},{1,5},{5,1},{2,6},{6,2},{3,7},{7,3},{8,12},{12,8},{9,1... | collective-permute-start | bytes 983048 | tf_op jit(solution)/shard_map/ppermute | solution.py:435
  138.1 2.2 %collective-permute-start.17 = (bf16[4,160,256]{2,1,0:T(8,128)(2,1)S(1)}, bf16[4,160,256]{2,1,0:T(8,128)(2,1)S(1)}, u32[]{:S(2)}, u32[]{:S(2)}) collective-permute-start(bf16[4,160,256]{2,1,0:T(8,128)(2,1)S(1)} %collective-permute-done.16.refs_14_), channel_id=1, source_target_pairs={{0,4},{4,0},{1,5},{5,1},{2,6},{6,2},{3,7},{7,3},{8,12},{12,8},{9,1... | collective-permute-start | bytes 983048 | tf_op jit(solution)/shard_map/ppermute | solution.py:435
  154.6 6.0 %collective-permute-start.18 = (bf16[32,2048]{1,0:T(8,128)(2,1)S(1)}, bf16[32,2048]{1,0:T(8,128)(2,1)S(1)}, u32[]{:S(2)}, u32[]{:S(2)}) collective-permute-start(bf16[32,2048]{1,0:T(8,128)(2,1)S(1)} %get-tuple-element.13), channel_id=1, source_target_pairs={{0,1},{1,2},{2,3},{3,0},{4,5},{5,6},{6,7},{7,4},{8,9},{9,10},{10,1... | collective-permute-start | bytes 393224 | tf_op jit(solution)/shard_map/ppermute | solution.py:458
  155.8 8.7 %collective-permute-start.19 = (bf16[32,2048]{1,0:T(8,128)(2,1)S(1)}, bf16[32,2048]{1,0:T(8,128)(2,1)S(1)}, u32[]{:S(2)}, u32[]{:S(2)}) collective-permute-start(bf16[32,2048]{1,0:T(8,128)(2,1)S(1)} %get-tuple-element.14), channel_id=1, source_target_pairs={{0,2},{1,3},{2,0},{3,1},{4,6},{5,7},{6,4},{7,5},{8,10},{9,11},{10,... | collective-permute-start | bytes 393224 | tf_op jit(solution)/shard_map/ppermute | solution.py:458
  158.5 6.0 %collective-permute-start.20 = (bf16[32,2048]{1,0:T(8,128)(2,1)S(1)}, bf16[32,2048]{1,0:T(8,128)(2,1)S(1)}, u32[]{:S(2)}, u32[]{:S(2)}) collective-permute-start(bf16[32,2048]{1,0:T(8,128)(2,1)S(1)} %get-tuple-element.15), channel_id=1, source_target_pairs={{0,3},{1,0},{2,1},{3,2},{4,7},{5,4},{6,5},{7,6},{8,11},{9,8},{10,9... | collective-permute-start | bytes 393224 | tf_op jit(solution)/shard_map/ppermute | solution.py:458
  (18 other events, 447.2 us)
